TPU v7x, 512 devices: a 8x2x16 block of a 8x8x16 slice. The times are simulated.
512 devices in a mesh: grp: 2 (over y), kv: 32 (over z, core), tp: 8 (over x).
Axes of the slice: x: 8, y: 2, z: 16, core: 2. Of those that a mesh axis runs over, the one named last changes fastest.
The devices are a block of a 8x8x16 slice.
Arguments:
- tokens: bfloat16 [256, 4096], P('grp', 'kv'), parts along dimension 0, may hold values from -16 to 16
- positions: int32 [256], P(('grp', 'kv')), parts along dimension 0, may hold values from 512 to 8191
- state: float32 [256, 16, 128, 128], P(('grp', 'kv'), 'tp'), parts along dimension 0, may hold values from -3 to 3
- norm_gain: float32 [4096], P('kv'), may hold values from 0.1 to 1.9
- w_query: bfloat16 [4096, 2048], P('kv', 'tp'), may hold values from -0.09375 to 0.09375
- w_key: bfloat16 [4096, 2048], P('kv', 'tp'), may hold values from -0.09375 to 0.09375
- w_value: bfloat16 [4096, 2048], P('kv', 'tp'), may hold values from -0.09375 to 0.09375
- w_gate: bfloat16 [4096, 2048], P('kv', 'tp'), may hold values from -0.09375 to 0.09375
- w_out: bfloat16 [2048, 4096], P('tp', 'kv'), may hold values from -0.125 to 0.125
- mlp_gain: float32 [4096], P('kv'), may hold values from 0.1 to 1.9
- w_up: bfloat16 [4096, 16384], P('kv', 'tp'), may hold values from -0.09375 to 0.09375
- w_down: bfloat16 [16384, 4096], P('tp', 'kv'), may hold values from -0.046875 to 0.046875
Outputs:
- layer_out: bfloat16 [256, 4096], P('grp', 'kv'), parts along dimension 0
- new_state: float32 [256, 16, 128, 128], P(('grp', 'kv'), 'tp'), parts along dimension 0
There are 2 independent parts, one for each index of `grp`. A program takes and returns all parts, laid end to end along the dimension named above; an argument that names none is the same for every part. Nothing has to cross between parts.
All inputs are finite; a program needn't handle non-finite values.
Results may differ from a plain program's by a relative error of at most 0.007.
Values may be sent and summed in bfloat16 or wider, within the bound.
A program may use at most 64 MiB of HBM per device.

v0:
```python
import math

import jax
import jax.numpy as jnp
from jax import lax
from jax.sharding import PartitionSpec as P

D = 4096
HEADS = 16


def cut_along(array, dim, count):
    dims = array.shape
    pieces = array.reshape(*dims[:dim], count, dims[dim] // count, *dims[dim + 1 :])
    return jnp.moveaxis(pieces, dim, 0)


def sent_and_summed(array, axis, dim):
    count = lax.axis_size(axis)
    pieces = lax.all_to_all(cut_along(array, dim, count), axis, 0, 0, tiled=True)
    return jnp.sum(pieces, axis=0)


def side_by_side(arrays, axis, dim, along):
    widths = [math.prod(a.shape[along:]) for a in arrays]
    both = jnp.concatenate(
        [a.reshape(*a.shape[:along], w) for a, w in zip(arrays, widths)], axis=along
    )
    filled = sent_and_summed(both, axis, dim)
    pieces = jnp.split(filled, [sum(widths[:k]) for k in range(1, len(widths))], axis=along)
    return tuple(
        (b.reshape(*filled.shape[:along], *a.shape[along:]) for a, b in zip(arrays, pieces))
    )


def joined_along(pieces, dim):
    dims = list(pieces.shape[1:])
    dims[dim] *= pieces.shape[0]
    return jnp.moveaxis(pieces, 0, dim).reshape(dims)


def from_everyone(array, axis):
    copies = jnp.broadcast_to(array, (lax.axis_size(axis), *array.shape))
    return lax.all_to_all(copies, axis, split_axis=0, concat_axis=0, tiled=True)


def gather_directly(array, axis, dim):
    return joined_along(from_everyone(array, axis), dim)


def over_copies(array, axis):
    everything = from_everyone(array, axis)
    return jnp.sum(everything, axis=0)


def turn(values, positions):
    half = values.shape[-1] // 2
    freq = 10000.0 ** (-(jnp.arange(half, dtype=jnp.float32) * 2.0) / values.shape[-1])
    angle = positions.astype(jnp.float32)[:, None, None] * freq[None, None, :]
    cosine = jnp.cos(angle)
    sine = jnp.sin(angle)
    first = values[..., :half]
    second = values[..., half:]
    return jnp.concatenate(
        [first * cosine - second * sine, first * sine + second * cosine], axis=-1
    )


def shards(
    tokens,
    positions,
    state,
    norm_gain,
    w_query,
    w_key,
    w_value,
    w_gate,
    w_out,
    mlp_gain,
    w_up,
    w_down,
):
    local_seqs, head_dev, head_size, _ = state.shape
    inputs = tokens.astype(jnp.float32)
    squares = jnp.sum(inputs * inputs, axis=1)
    normed = (inputs * norm_gain).astype(jnp.bfloat16)
    terms = jnp.stack(
        [
            jnp.dot(normed, weight, preferred_element_type=jnp.float32)
            for weight in (w_query, w_key, w_value, w_gate)
        ],
        axis=1,
    )
    summed, total_sq = side_by_side((terms, squares), "kv", 0, 1)
    scale1 = lax.rsqrt(total_sq / D + 1e-06)
    summed = (summed * scale1[:, None, None]).reshape(local_seqs, 4, head_dev, head_size)
    query = turn(summed[:, 0], positions)
    key_rows = turn(summed[:, 1], positions) * head_size ** (-0.5)
    value = summed[:, 2]
    gate = summed[:, 3]
    heads = (lax.axis_index("tp") * head_dev + jnp.arange(head_dev)).astype(jnp.float32)
    gamma = 1.0 - 2.0 ** (-5.0 - 5.0 * heads / (HEADS - 1))
    new_state = gamma[None, :, None, None] * state + key_rows[:, :, :, None] * value[:, :, None, :]
    read = jnp.einsum("bhd,bhde->bhe", query, new_state, precision=lax.Precision.HIGHEST)
    read = read * lax.rsqrt(jnp.mean(read * read, axis=-1, keepdims=True) + 1e-06)
    retained = (
        (read * jax.nn.silu(gate)).reshape(local_seqs, head_dev * head_size).astype(jnp.bfloat16)
    )
    head_terms = jnp.dot(
        gather_directly(retained, "kv", 0), w_out, preferred_element_type=jnp.float32
    )
    mixed = (inputs + over_copies(head_terms, "tp")).astype(jnp.bfloat16)
    middle = mixed.astype(jnp.float32)
    squares2 = jnp.sum(middle * middle, axis=1)
    normed2 = (middle * mlp_gain).astype(jnp.bfloat16)
    upward = jnp.dot(normed2, w_up, preferred_element_type=jnp.float32)
    up_rows, row_sq2 = side_by_side((upward, squares2), "kv", 0, 1)
    scale2 = lax.rsqrt(row_sq2 / D + 1e-06)
    hidden_rows = jnp.square(jax.nn.relu(up_rows * scale2[:, None])).astype(jnp.bfloat16)
    down_terms = jnp.dot(
        gather_directly(hidden_rows, "kv", 0), w_down, preferred_element_type=jnp.float32
    )
    layer_out = (middle + over_copies(down_terms, "tp")).astype(jnp.bfloat16)
    return (layer_out, new_state)


def solution(mesh):
    return jax.shard_map(
        shards,
        mesh=mesh,
        in_specs=(
            P("grp", "kv"),
            P(("grp", "kv")),
            P(("grp", "kv"), "tp", None, None),
            P("kv"),
            P("kv", "tp"),
            P("kv", "tp"),
            P("kv", "tp"),
            P("kv", "tp"),
            P("tp", "kv"),
            P("kv"),
            P("kv", "tp"),
            P("tp", "kv"),
        ),
        out_specs=(P("grp", "kv"), P(("grp", "kv"), "tp", None, None)),
        check_vma=False,
    )
```

profile of v0, /device:TPU:65, one launch (start us, length us, event | category | flops | bytes accessed | tf_op | source)
XLA Modules:
  0.0 253.8 jit_solution(2219122011889338196)
XLA Ops:
  0.6 0.9 fusion.1
  1.6 0.3 concatenate.34
  1.8 1.0 convolution_bitcast_fusion.3
  2.9 1.0 convolution_bitcast_fusion.2
  3.9 1.0 convolution_bitcast_fusion.1
  4.9 1.0 convolution_bitcast_fusion
  6.0 0.3 copy.31
  6.3 0.4 concatenate.26
  6.7 0.9 pad_maximum_fusion.1
  7.7 45.3 %all-to-all-start = ((f32[32,4,1025]{2,1,0:T(4,128)}), f32[32,4,1025]{2,1,0:T(4,128)S(1)}, u32[]{:S(2)}, u32[]{:S(2)}) async-start(f32[32,4,1025]{2,1,0:T(4,128)} %pad_maximum_fusion.1), calls=%async_computation | async-start | bytes 1179648 | tf_op jit(solution)/shard_map/all_to_all | solution.py:20
  53.1 0.1 multiply_cosine_fusion
  53.2 36.0 %all-to-all-done = f32[32,4,1025]{2,1,0:T(4,128)S(1)} async-done(((f32[32,4,1025]{2,1,0:T(4,128)}), f32[32,4,1025]{2,1,0:T(4,128)S(1)}, u32[]{:S(2)}, u32[]{:S(2)}) %all-to-all-start) | async-done | bytes 524832 | tf_op jit(solution)/shard_map/all_to_all | solution.py:20
  89.3 0.1 fusion.23
  89.7 0.2 multiply_add_fusion
  90.0 0.5 fusion.26
  90.7 17.1 %all_to_all.30 = bf16[32,4,256]{2,1,0:T(4,128)(2,1)S(1)} all-to-all(bf16[32,4,256]{2,1,0:T(4,128)(2,1)S(1)} %broadcast_in_dim.8), channel_id=1, replica_groups=mesh['grp'=2,'kv'=32,'tp'=8] {'kv'}, dimensions={0} | all-to-all | bytes 131072 | tf_op jit(solution)/shard_map/all_to_all | solution.py:44
  107.8 0.1 fusion.27
  108.0 21.9 %all_to_all.31 = f32[8,128,128]{2,1,0:T(8,128)S(1)} all-to-all(f32[8,128,128]{2,1,0:T(8,128)S(1)} %broadcast_in_dim.9), channel_id=1, replica_groups=mesh['grp'=2,'kv'=32,'tp'=8] {'tp'}, dimensions={0} | all-to-all | bytes 1048576 | tf_op jit(solution)/shard_map/all_to_all | solution.py:44
  130.0 0.1 fusion.4
  130.1 0.3 concatenate.35
  130.4 0.3 fusion.6
  130.7 0.3 concatenate.31
  131.0 0.2 pad_maximum_fusion
  131.2 64.6 %all_to_all.32 = f32[32,4,2049]{2,1,0:T(4,128)S(1)} all-to-all(f32[32,4,2049]{2,1,0:T(4,128)S(1)} %pad_maximum_fusion), channel_id=1, replica_groups=mesh['grp'=2,'kv'=32,'tp'=8] {'kv'}, dimensions={0} | all-to-all | bytes 2098176 | tf_op jit(solution)/shard_map/all_to_all | solution.py:20
  195.9 0.2 reduce_sum.68
  196.1 0.1 fusion.20
  196.3 0.2 broadcast_in_dim.10
  196.5 37.3 %all_to_all.33 = bf16[32,4,2048]{2,1,0:T(4,128)(2,1)S(1)} all-to-all(bf16[32,4,2048]{2,1,0:T(4,128)(2,1)S(1)} %broadcast_in_dim.10), channel_id=1, replica_groups=mesh['grp'=2,'kv'=32,'tp'=8] {'kv'}, dimensions={0} | all-to-all | bytes 1048576 | tf_op jit(solution)/shard_map/all_to_all | solution.py:44
  233.8 0.1 reshape.141
  233.9 0.3 fusion.28
  234.3 18.9 %all_to_all.34 = f32[8,128,128]{2,1,0:T(8,128)S(1)} all-to-all(f32[8,128,128]{2,1,0:T(8,128)S(1)} %broadcast_in_dim.11), channel_id=1, replica_groups=mesh['grp'=2,'kv'=32,'tp'=8] {'tp'}, dimensions={0} | all-to-all | bytes 1048576 | tf_op jit(solution)/shard_map/all_to_all | solution.py:44
  253.2 0.6 fusion.5
  (38 shorter events, 0.9 us)
Async XLA Ops:
  0.6 129.7 %copy-start = (bf16[128,2048]{1,0:T(8,128)(2,1)S(1)}, bf16[128,2048]{1,0:T(8,128)(2,1)}, u32[]{:S(2)}) copy-start(bf16[128,2048]{1,0:T(8,128)(2,1)} %param.22) | copy-start | bytes 1572868
  6.7 46.3 %copy-start.7 = (s32[4]{0:T(128)S(1)}, s32[4]{0:T(128)}, u32[]{:S(2)}) copy-start(s32[4]{0:T(128)} %param.13) | copy-start | bytes 52
  7.7 82.1 %copy-start.4 = (f32[4,2,128,128]{3,2,1,0:T(8,128)S(1)}, f32[4,2,128,128]{3,2,1,0:T(8,128)}, u32[]{:S(2)}) copy-start(f32[4,2,128,128]{3,2,1,0:T(8,128)} %param.14) | copy-start | bytes 1572868
  7.7 81.5 %all-to-all-start = ((f32[32,4,1025]{2,1,0:T(4,128)}), f32[32,4,1025]{2,1,0:T(4,128)S(1)}, u32[]{:S(2)}, u32[]{:S(2)}) async-start(f32[32,4,1025]{2,1,0:T(4,128)} %pad_maximum_fusion.1), calls=%async_computation | async-start | bytes 1179648 | tf_op jit(solution)/shard_map/all_to_all | solution.py:20
  89.3 18.5 %copy-start.5 = (bf16[256,128]{1,0:T(8,128)(2,1)S(1)}, bf16[256,128]{1,0:T(8,128)(2,1)}, u32[]{:S(2)}) copy-start(bf16[256,128]{1,0:T(8,128)(2,1)} %param.20) | copy-start | bytes 196612
  89.9 40.0 %copy-start.1 = (f32[4,2,128,128]{3,2,1,0:T(8,128)}, f32[4,2,128,128]{3,2,1,0:T(8,128)S(1)}, u32[]{:S(2)}) copy-start(f32[4,2,128,128]{3,2,1,0:T(8,128)S(1)} %multiply_add_fusion) | copy-start | bytes 1572868
  108.0 22.0 %copy-start.2 = (bf16[128,128]{1,0:T(8,128)(2,1)S(1)}, bf16[128,128]{1,0:T(8,128)(2,1)}, u32[]{:S(2)}) copy-start(bf16[128,128]{1,0:T(8,128)(2,1)} %param.12) | copy-start | bytes 98308
  108.0 22.4 %copy-start.6 = (f32[128]{0:T(128)S(1)}, f32[128]{0:T(128)}, u32[]{:S(2)}) copy-start(f32[128]{0:T(128)} %param.21) | copy-start | bytes 1540
  196.5 37.4 %copy-start.3 = (bf16[2048,128]{1,0:T(8,128)(2,1)S(1)}, bf16[2048,128]{1,0:T(8,128)(2,1)}, u32[]{:S(2)}) copy-start(bf16[2048,128]{1,0:T(8,128)(2,1)} %param.23) | copy-start | bytes 1572868
where the time goes:
time: 255 us; the launch traced here: 254 us
  blocking collectives  160 us (63%)
  starting transfers between devices  45.3 us (18%)
  waiting for transfers between devices  36 us (14%)
  matrix products  5.31 us (2%)
  other arithmetic  4.31 us (2%)
    all_to_all x4, blocking collectives, from_everyone(): return lax.all_to_all(copies, axis, split_axis=0, concat_axis=0, tiled=True)  95.2 us
    all_to_all x1, blocking collectives, sent_and_summed(): lax.all_to_all(cut_along(array, dim, count), axis, 0, 0, tiled=True)  64.6 us
    all_to_all x1, starting transfers between devices, sent_and_summed(): lax.all_to_all(cut_along(array, dim, count), axis, 0, 0, tiled=True)  45.3 us
    all_to_all x1, waiting for transfers between devices, sent_and_summed(): lax.all_to_all(cut_along(array, dim, count), axis, 0, 0, tiled=True)  36 us
  transfers between devices with their start and end apart: 1, of which 1 were waited for; matrix products, arithmetic and copies ran while one was open for 0% of the time, Pallas kernels for 0%

commit v1 on v0

v1 whole, which is shorter than its diff:
```python
import functools

import jax
import jax.numpy as jnp
import numpy as np
from jax import lax
from jax.experimental import pallas as pl
from jax.experimental.pallas import tpu as pltpu
from jax.sharding import PartitionSpec as P

MESH = pl.DeviceIdType.MESH
F32 = jnp.float32
BF16 = jnp.bfloat16
EPS = 1e-06


def far_first(step, count):
    swing = (step + 1) // 2
    return count // 2 + swing * (2 * (step % 2) - 1)


def kernel(
    cfg,
    pos_ref,
    x_hbm,
    state_hbm,
    gain_hbm,
    wq_hbm,
    wk_hbm,
    wv_hbm,
    wg_hbm,
    wo_hbm,
    gain2_hbm,
    wu_hbm,
    wd_hbm,
    freq_ref,
    out_ref,
    state_out,
    x_in,
    gain_in,
    w_in,
    state_in,
    state_new,
    wo_in,
    wu_in,
    wd_in,
    tok2,
    gain2,
    part,
    swap_s,
    swap_r,
    sq_s,
    sq_r,
    send_a,
    recv_a,
    ret_s,
    ret_r,
    ret_f,
    send_c,
    recv_c,
    tok_rows,
    mix_s,
    mix_r,
    sq2_s,
    sq2_r,
    send_d,
    recv_d,
    hid_s,
    hid_r,
    out_s,
    out_r,
    load_sem,
    send_sem,
    recv_sem,
):
    nk, nt, nz, d_model, heads_all = cfg
    me = lax.axis_index("kv")
    tp = lax.axis_index("tp")
    z = me // 2
    c = me % 2
    mate = me + 1 - 2 * c
    block = tp * 2 + c
    nb = nt * 2
    rows = x_in.shape[0]
    width = x_in.shape[1]
    seqs = rows // nk
    per_chip = rows // nz
    size = width
    half_ff = wu_in.shape[1]

    def kv_peer(step):
        chip = lax.rem(z + far_first(step // 2, nz), nz)
        other = lax.rem(c + step % 2, 2)
        last = (step == nk - 2).astype(jnp.int32)
        return last * mate + (1 - last) * (chip * 2 + other)

    def chip_peer(step):
        return lax.rem(z + far_first(step, nz), nz) * 2 + c

    def block_peer(step):
        chip = lax.rem(tp + far_first(step // 2, nt), nt)
        other = lax.rem(c + step % 2, 2)
        last = (step == nb - 2).astype(jnp.int32)
        return last * tp + (1 - last) * chip, last * (1 - c) + (1 - last) * other

    def each(count, body):
        lax.fori_loop(0, count, lambda i, carry: (body(i), carry)[1], 0)

    barrier = pltpu.get_barrier_semaphore()

    def greet_kv(i):
        pl.semaphore_signal(barrier, inc=1, device_id={"kv": kv_peer(i)}, device_id_type=MESH)

    def greet_block(i):
        t, core = block_peer(i)
        pl.semaphore_signal(
            barrier, inc=1, device_id={"kv": z * 2 + core, "tp": t}, device_id_type=MESH
        )

    each(nk - 1, greet_kv)
    each(nb - 2, greet_block)

    def load(src, dst, sem):
        copy = pltpu.make_async_copy(src, dst, load_sem.at[sem])
        copy.start()
        return copy

    first = [
        load(x_hbm, x_in, 0),
        load(gain_hbm, gain_in, 1),
        load(wq_hbm, w_in.at[0], 2),
        load(wk_hbm, w_in.at[1], 3),
        load(wv_hbm, w_in.at[2], 4),
        load(wg_hbm, w_in.at[3], 5),
    ]
    here = pl.ds(pl.multiple_of(c * half_ff, 128), half_ff)
    there = pl.ds(pl.multiple_of((1 - c) * half_ff, 128), half_ff)
    mine = pl.ds(pl.multiple_of(c * size, 128), size)
    other_head = pl.ds(pl.multiple_of((1 - c) * size, 128), size)
    my_rows = pl.ds(pl.multiple_of(c * width, 128), width)
    later = [
        load(state_hbm, state_in, 6),
        load(wo_hbm.at[mine], wo_in.at[:, my_rows], 7),
        load(gain2_hbm, gain2.at[:, my_rows], 8),
        load(wu_hbm.at[:, here], wu_in.at[my_rows], 9),
        load(wd_hbm.at[here], wd_in.at[:, my_rows], 10),
    ]

    for copy in first:
        copy.wait()
    x = x_in[...].astype(F32)
    normed = (x * gain_in[...]).astype(BF16)
    square = x * x
    sq_s[...] = jnp.sum(jnp.transpose(square), axis=0, keepdims=True)
    sq_r[me] = sq_s[...]
    for n in range(4):
        both = jnp.dot(normed, w_in[n], preferred_element_type=F32)
        part[0, :, n * size : (n + 1) * size] = both[:, :size]
        part[1, :, n * size : (n + 1) * size] = both[:, size:]
    swap_s[...] = part[1 - c].astype(BF16)
    tok2[c] = x_in[...]

    pl.semaphore_wait(barrier, nk - 1 + nb - 2)

    def remote(src, dst, phase, kv, t=None):
        where = {"kv": kv} if t is None else {"kv": kv, "tp": t}
        pltpu.make_async_remote_copy(
            src_ref=src,
            dst_ref=dst,
            send_sem=send_sem.at[phase],
            recv_sem=recv_sem.at[phase],
            device_id=where,
            device_id_type=MESH,
        ).start()

    def arrived(ref, phase):
        pltpu.make_async_copy(ref, ref, recv_sem.at[phase]).wait()

    def left(ref, phase):
        pltpu.make_async_copy(ref, ref, send_sem.at[phase]).wait()

    remote(swap_s, swap_r, 0, mate)

    def send_squares(i):
        remote(sq_s, sq_r.at[me], 1, kv_peer(i))

    each(nk - 1, send_squares)
    remote(x_in, tok2.at[c], 2, mate)
    remote(gain2_hbm, gain2.at[:, my_rows], 3, mate)
    remote(wo_hbm.at[other_head], wo_in.at[:, my_rows], 4, mate)
    remote(wu_hbm.at[:, there], wu_in.at[my_rows], 5, mate)
    remote(wd_hbm.at[there], wd_in.at[:, my_rows], 6, mate)

    arrived(swap_r, 0)
    part[c] = part[c] + swap_r[...].astype(F32)
    for j in range(nk):
        send_a[j] = part[c, j * seqs : (j + 1) * seqs, :].astype(BF16)
    recv_a[me] = send_a[me]

    def send_terms(i):
        peer = kv_peer(i)
        remote(send_a.at[peer], recv_a.at[me], 7, peer)

    each(nk - 1, send_terms)

    row = lax.broadcasted_iota(jnp.int32, (seqs, size), 0)
    lane = lax.broadcasted_iota(jnp.int32, (seqs, size), 1)
    place = jnp.zeros((seqs, size), F32)
    for i in range(seqs):
        place = jnp.where(row == i, pos_ref[i].astype(F32), place)
    angle = place * freq_ref[...]
    cosine = jnp.cos(angle)
    sine = jnp.sin(angle)
    sine = jnp.where(lane < size // 2, -sine, sine)
    later[0].wait()

    arrived(sq_r.at[pl.ds(0, nk - 1)], 1)
    total_sq = jnp.sum(sq_r[...], axis=0)
    row_sq = jnp.sum(jnp.where(lane == row + me * seqs, total_sq, 0.0), axis=1, keepdims=True)
    scale1 = lax.rsqrt(row_sq / d_model + EPS)

    arrived(recv_a.at[pl.ds(0, nk - 1)], 7)
    queries, keys, values, gates = [], [], [], []

    def turn(v):
        return v * cosine + pltpu.roll(v, size // 2, 1) * sine

    for h in range(2):
        total = recv_a[h].astype(F32)
        for j in range(1, nz):
            total = total + recv_a[2 * j + h].astype(F32)
        total = total * scale1
        queries.append(turn(total[:, :size]))
        keys.append(turn(total[:, size : 2 * size]) * size**-0.5)
        values.append(total[:, 2 * size : 3 * size])
        gates.append(total[:, 3 * size :])
    pad = jnp.zeros((size - 4 * seqs, size), F32)
    columns = jnp.transpose(jnp.concatenate(queries + keys + [pad], axis=0))
    for h in range(2):
        head = (tp * 2 + h).astype(F32)
        power = jnp.full((1, size), -5.0, F32) - 5.0 * head / (heads_all - 1)
        gamma = 1.0 - jnp.exp2(power)
        reads = []
        for i in range(seqs):
            at = h * seqs + i
            new = (
                gamma * state_in[i, h]
                + columns[:, 2 * seqs + at : 2 * seqs + at + 1] * values[h][i : i + 1]
            )
            state_new[i, h] = new
            reads.append(jnp.sum(columns[:, at : at + 1] * new, axis=0, keepdims=True))
        read = jnp.concatenate(reads, axis=0)
        read = read * lax.rsqrt(jnp.mean(read * read, axis=1, keepdims=True) + EPS)
        gate = gates[h]
        ret_s[h] = (read * (gate / (1.0 + jnp.exp(-gate)))).astype(BF16)
    ret_r[me] = ret_s[c]

    def send_retained(i):
        peer = kv_peer(i)
        remote(ret_s.at[peer % 2], ret_r.at[me], 8, peer)

    each(nk - 1, send_retained)
    state_copy = load(state_new, state_out, 11)

    later[1].wait()
    later[2].wait()
    arrived(tok2.at[0], 2)
    arrived(gain2.at[:, pl.ds(0, width)], 3)
    arrived(wo_in.at[:, pl.ds(0, width)], 4)
    for m in range(nb):
        for s in range(2):
            tok_rows[m, :, s * width : (s + 1) * width] = tok2[
                s, m * per_chip : (m + 1) * per_chip
            ].astype(F32)

    arrived(ret_r.at[pl.ds(0, nk - 1)], 8)
    for j in range(nk):
        ret_f[j * seqs : (j + 1) * seqs] = ret_r[j].astype(F32)
    terms = jnp.dot(ret_f[...].astype(BF16), wo_in[...], preferred_element_type=F32)
    send_c[0] = terms.reshape(nb, per_chip, 2 * width).astype(BF16)
    recv_c[0, block] = send_c[0, block]

    def send_sums(which, phase):
        def send(i):
            t, core = block_peer(i)
            remote(send_c.at[which, t * 2 + core], recv_c.at[which, block], phase, z * 2 + core, t)

        each(nb - 1, send)

    send_sums(0, 9)
    arrived(recv_c.at[0, pl.ds(0, nb - 1)], 9)
    mixed = (tok_rows[block] + jnp.sum(recv_c[0].astype(F32), axis=0)).astype(BF16)
    mix_s[...] = mixed
    mix_r[block] = mixed

    def send_mixed(i):
        t, core = block_peer(i)
        remote(mix_s, mix_r.at[block], 10, z * 2 + core, t)

    each(nb - 1, send_mixed)
    later[3].wait()
    arrived(wu_in.at[pl.ds(0, width)], 5)
    arrived(mix_r.at[pl.ds(0, nb - 1)], 10)
    middle = mix_r[...].astype(F32).reshape(rows, 2 * width)
    square = middle * middle
    sq2_s[...] = jnp.sum(
        jnp.transpose(square[:, :width] + square[:, width:]), axis=0, keepdims=True
    )
    sq2_r[z] = sq2_s[...]

    def send_squares2(i):
        remote(sq2_s, sq2_r.at[z], 11, chip_peer(i))

    each(nz - 1, send_squares2)
    normed2 = (middle * gain2[...]).astype(BF16)
    upward = jnp.dot(normed2, wu_in[...], preferred_element_type=F32)
    send_d[...] = upward.reshape(nz, per_chip, half_ff).astype(BF16)
    recv_d[z] = send_d[z]

    def send_up(i):
        peer = chip_peer(i)
        remote(send_d.at[peer // 2], recv_d.at[z], 12, peer)

    each(nz - 1, send_up)
    row = lax.broadcasted_iota(jnp.int32, (per_chip, size), 0)
    lane = lax.broadcasted_iota(jnp.int32, (per_chip, size), 1)
    arrived(sq2_r.at[pl.ds(0, nz - 1)], 11)
    total_sq = jnp.sum(sq2_r[...], axis=0)
    row_sq = jnp.sum(jnp.where(lane == row + z * per_chip, total_sq, 0.0), axis=1, keepdims=True)
    scale2 = lax.rsqrt(row_sq / d_model + EPS)
    arrived(recv_d.at[pl.ds(0, nz - 1)], 12)
    total = recv_d[0].astype(F32)
    for j in range(1, nz):
        total = total + recv_d[j].astype(F32)
    hidden = jnp.maximum(total * scale2, 0.0)
    hid_s[...] = (hidden * hidden).astype(BF16)
    hid_r[z] = hid_s[...]

    def send_hidden(i):
        remote(hid_s, hid_r.at[z], 13, chip_peer(i))

    each(nz - 1, send_hidden)
    later[4].wait()
    arrived(wd_in.at[:, pl.ds(0, width)], 6)
    arrived(hid_r.at[pl.ds(0, nz - 1)], 13)
    hidden_all = hid_r[...].astype(F32).reshape(rows, half_ff).astype(BF16)
    terms = jnp.dot(hidden_all, wd_in[...], preferred_element_type=F32)
    send_c[1] = terms.reshape(nb, per_chip, 2 * width).astype(BF16)
    recv_c[1, block] = send_c[1, block]
    send_sums(1, 14)
    arrived(recv_c.at[1, pl.ds(0, nb - 1)], 14)
    final = (mix_s[...].astype(F32) + jnp.sum(recv_c[1].astype(F32), axis=0)).astype(BF16)
    for s in range(2):
        out_s[s] = final[:, s * width : (s + 1) * width]
    out_r[block] = out_s[c]

    def send_out(i):
        t, core = block_peer(i)
        remote(out_s.at[core], out_r.at[block], 15, z * 2 + core, t)

    each(nb - 1, send_out)

    state_copy.wait()
    left(swap_s, 0)
    left(sq_r.at[pl.ds(0, nk - 1)], 1)
    left(x_in, 2)
    left(gain_in, 3)
    left(w_in.at[0, :, pl.ds(0, width)], 4)
    left(wu_in.at[pl.ds(0, width)], 5)
    left(wd_in.at[:, pl.ds(0, width)], 6)
    left(send_a.at[pl.ds(0, nk - 1)], 7)
    left(ret_r.at[pl.ds(0, nk - 1)], 8)
    left(send_c.at[0, pl.ds(0, nb - 1)], 9)
    left(mix_r.at[pl.ds(0, nb - 1)], 10)
    left(sq2_r.at[pl.ds(0, nz - 1)], 11)
    left(send_d.at[pl.ds(0, nz - 1)], 12)
    left(hid_r.at[pl.ds(0, nz - 1)], 13)
    left(send_c.at[1, pl.ds(0, nb - 1)], 14)
    left(out_r.at[pl.ds(0, nb - 1)], 15)
    arrived(out_r.at[pl.ds(0, nb - 1)], 15)
    out_ref[...] = out_r[...].astype(F32).reshape(rows, width).astype(BF16)


def solution(mesh):
    nk, nt = mesh.shape["kv"], mesh.shape["tp"]
    nz = nk // 2

    def shards(
        tokens,
        positions,
        state,
        norm_gain,
        w_query,
        w_key,
        w_value,
        w_gate,
        w_out,
        mlp_gain,
        w_up,
        w_down,
    ):
        rows, width = tokens.shape
        seqs, heads, size, _ = state.shape
        ff = w_up.shape[1]
        per_chip = rows // nz
        nb = 2 * nt
        inverse = 10000.0 ** (-(np.arange(size // 2, dtype=np.float64) * 2.0) / size)
        freq = jnp.asarray(np.concatenate([inverse, inverse])[None, :].astype(np.float32))
        cfg = (nk, nt, nz, width * nk, heads * nt)
        anywhere = pl.BlockSpec(memory_space=pl.ANY)
        vmem = pl.BlockSpec(memory_space=pltpu.VMEM)
        smem = pl.BlockSpec(memory_space=pltpu.SMEM)
        scratch = [
            ((rows, width), BF16),
            ((1, width), F32),
            ((4, width, heads * size), BF16),
            (state.shape, F32),
            (state.shape, F32),
            ((size, 2 * width), BF16),
            ((2 * width, ff // 2), BF16),
            ((ff // 2, 2 * width), BF16),
            ((2, rows, width), BF16),
            ((1, 2 * width), F32),
            ((2, rows, 4 * size), F32),
            ((rows, 4 * size), BF16),
            ((rows, 4 * size), BF16),
            ((1, rows), F32),
            ((nk, 1, rows), F32),
            ((nk, seqs, 4 * size), BF16),
            ((nk, seqs, 4 * size), BF16),
            ((2, seqs, size), BF16),
            ((nk, seqs, size), BF16),
            ((rows, size), F32),
            ((2, nb, per_chip, 2 * width), BF16),
            ((2, nb, per_chip, 2 * width), BF16),
            ((nb, per_chip, 2 * width), F32),
            ((per_chip, 2 * width), BF16),
            ((nb, per_chip, 2 * width), BF16),
            ((1, rows), F32),
            ((nz, 1, rows), F32),
            ((nz, per_chip, ff // 2), BF16),
            ((nz, per_chip, ff // 2), BF16),
            ((per_chip, ff // 2), BF16),
            ((nz, per_chip, ff // 2), BF16),
            ((2, per_chip, width), BF16),
            ((nb, per_chip, width), BF16),
        ]
        return pl.pallas_call(
            functools.partial(kernel, cfg),
            out_shape=(
                jax.ShapeDtypeStruct((rows, width), BF16),
                jax.ShapeDtypeStruct(state.shape, F32),
            ),
            in_specs=[smem] + [anywhere] * 11 + [vmem],
            out_specs=(vmem, anywhere),
            scratch_shapes=[pltpu.VMEM(s, t) for s, t in scratch]
            + [
                pltpu.SemaphoreType.DMA((12,)),
                pltpu.SemaphoreType.DMA((16,)),
                pltpu.SemaphoreType.DMA((16,)),
            ],
            compiler_params=pltpu.CompilerParams(
                collective_id=0, has_side_effects=True, vmem_limit_bytes=40 * 1024 * 1024
            ),
            name="step",
        )(
            positions,
            tokens,
            state,
            norm_gain.reshape(1, width),
            w_query,
            w_key,
            w_value,
            w_gate,
            w_out,
            mlp_gain.reshape(1, width),
            w_up,
            w_down,
            freq,
        )

    return jax.shard_map(
        shards,
        mesh=mesh,
        in_specs=(
            P("grp", "kv"),
            P(("grp", "kv")),
            P(("grp", "kv"), "tp", None, None),
            P("kv"),
            P("kv", "tp"),
            P("kv", "tp"),
            P("kv", "tp"),
            P("kv", "tp"),
            P("tp", "kv"),
            P("kv"),
            P("kv", "tp"),
            P("tp", "kv"),
        ),
        out_specs=(P("grp", "kv"), P(("grp", "kv"), "tp", None, None)),
        check_vma=False,
    )
```

time: 255 us -> 127 us (0.50)
  blocking collectives: 160 us -> 0 us
  Pallas kernels: 0 us -> 116 us
  starting transfers between devices: 45.3 us -> 0 us
  waiting for transfers between devices: 36 us -> 0 us
  local copies, waits for them, and re-layouts: 2.09 us -> 10.2 us
  matrix products: 5.31 us -> 0 us
  other arithmetic: 4.31 us -> 0 us
    all_to_all x5 -> x0, blocking collectives: 160 us -> none  [the longest x4 95.2 us: from_everyone(): return lax.all_to_all(copies, axis, split_axis=0, concat_axis=0, tiled=True)]
    pallas_call x0 -> x1, Pallas kernels: none -> 116 us  [shards(): pl.pallas_call(functools.partial(kernel, cfg), out_shape=(jax.ShapeDtypeS...]
    all_to_all x1 -> x0, starting transfers between devices: 45.3 us -> none  [sent_and_summed(): lax.all_to_all(cut_along(array, dim, count), axis, 0, 0, tiled=True)]
    all_to_all x1 -> x0, waiting for transfers between devices: 36 us -> none  [sent_and_summed(): lax.all_to_all(cut_along(array, dim, count), axis, 0, 0, tiled=True)]
    unnamed x17 -> x28, local copies, waits for them, and re-layouts: 0.06 us -> 10.2 us
    dot_general x8 -> x0, matrix products: 5.31 us -> none  [the longest x4 4.08 us: shards(): jnp.dot(normed, weight, preferred_element_type=jnp.float32)]
  transfers between devices with their start and end apart: 1 -> 0, of which waited for: 1 -> 0; matrix products, arithmetic and copies ran while one was open for 0% -> 0% of each run, Pallas kernels for 0% -> 0%
where the time goes in v1:
time: 127 us
  Pallas kernels  116 us (91%)
  local copies, waits for them, and re-layouts  10.2 us (8%)
    pallas_call x1, Pallas kernels, shards(): pl.pallas_call(functools.partial(kernel, cfg), out_shape=(jax.ShapeDtypeS...  116 us
    unnamed x28, local copies, waits for them, and re-layouts  10.2 us

profile of v1, /device:TPU:65, one launch (start us, length us, event | category | flops | bytes accessed | tf_op | source)
XLA Modules:
  0.0 126.7 jit_solution(6258549763269082520)
XLA Ops:
  0.6 0.0 copy-start.12
  0.6 0.0 copy-start.9
  0.7 0.0 copy-start.10
  0.7 0.0 copy-start.11
  0.7 0.6 copy-done.12
  1.3 0.0 copy-done.9
  1.3 0.0 copy-done.10
  1.3 0.0 copy-done.11
  1.3 0.0 copy-start
  1.3 1.0 copy-done
  2.4 0.0 copy-start.1
  2.4 1.0 copy-done.1
  3.4 0.0 copy-start.2
  3.4 1.0 copy-done.2
  4.5 0.0 copy-start.3
  4.5 0.8 copy-done.3
  5.3 0.0 copy-start.4
  5.3 0.8 copy-done.4
  6.1 0.0 copy-start.5
  6.1 0.8 copy-done.5
  7.0 0.0 copy-start.6
  7.0 0.8 copy-done.6
  7.8 0.0 copy-start.7
  7.8 0.8 copy-done.7
  8.7 0.0 copy-start.8
  8.7 0.8 copy-done.8
  9.4 115.8 %step.1 = (bf16[128,128]{1,0:T(8,128)(2,1)S(1)}, f32[4,2,128,128]{3,2,1,0:T(8,128)S(1)}) custom-call(s32[4]{0:T(128)S(1)} %copy-done.9, bf16[128,128]{1,0:T(8,128)(2,1)S(1)} %copy-done.8, f32[4,2,128,128]{3,2,1,0:T(8,128)S(1)} %copy-done, f32[1,128]{1,0:T(1,128)S(1)} %bitcast.2, bf16[128,256]{1,0:T(8,128)(2,1)S(1)} %copy-done.3, ...), custom_call_target="tpu_custom_call" | custom-call | tf_op jit(solution)/shard_map/step/pallas_call | solution.py:448
  125.3 0.6 copy.17
  125.9 0.8 copy.18
Async XLA Ops:
  0.6 0.7 copy-start.12
  0.6 0.7 copy-start.9
  0.7 0.7 copy-start.10
  0.7 0.7 copy-start.11
  1.3 1.0 copy-start
  2.4 1.0 copy-start.1
  3.4 1.0 copy-start.2
  4.5 0.8 copy-start.3
  5.3 0.8 copy-start.4
  6.1 0.8 copy-start.5
  7.0 0.8 copy-start.6
  7.8 0.8 copy-start.7
  8.7 0.8 copy-start.8

commit v2 on v1

--- a/solution.py
+++ b/solution.py
@@ -162,6 +162,8 @@
 
     pl.semaphore_wait(barrier, nk - 1 + nb - 2)
 
+    going, coming = {}, {}
+
     def remote(src, dst, phase, kv, t=None):
         where = {"kv": kv} if t is None else {"kv": kv, "tp": t}
         pltpu.make_async_remote_copy(
@@ -173,25 +175,37 @@
             device_id_type=MESH,
         ).start()
 
-    def arrived(ref, phase):
+    def to_mate(src, dst, phase, amount):
+        remote(src, dst, phase, mate)
+        going[phase] = coming[phase] = amount
+
+    def to_each(count, phase, amount, send):
+        each(count, send)
+        going[phase] = coming[phase] = amount.at[pl.ds(0, count)]
+
+    def arrived(phase):
+        ref = coming.pop(phase)
         pltpu.make_async_copy(ref, ref, recv_sem.at[phase]).wait()
 
-    def left(ref, phase):
-        pltpu.make_async_copy(ref, ref, send_sem.at[phase]).wait()
-
-    remote(swap_s, swap_r, 0, mate)
+    def finish():
+        for phase in list(coming):
+            arrived(phase)
+        for phase, ref in going.items():
+            pltpu.make_async_copy(ref, ref, send_sem.at[phase]).wait()
+
+    to_mate(swap_s, swap_r, 0, swap_r)
 
     def send_squares(i):
         remote(sq_s, sq_r.at[me], 1, kv_peer(i))
 
-    each(nk - 1, send_squares)
-    remote(x_in, tok2.at[c], 2, mate)
-    remote(gain2_hbm, gain2.at[:, my_rows], 3, mate)
-    remote(wo_hbm.at[other_head], wo_in.at[:, my_rows], 4, mate)
-    remote(wu_hbm.at[:, there], wu_in.at[my_rows], 5, mate)
-    remote(wd_hbm.at[there], wd_in.at[:, my_rows], 6, mate)
-
-    arrived(swap_r, 0)
+    to_each(nk - 1, 1, sq_r, send_squares)
+    to_mate(x_in, tok2.at[c], 2, x_in)
+    to_mate(gain2_hbm, gain2.at[:, my_rows], 3, gain_in)
+    to_mate(wo_hbm.at[other_head], wo_in.at[:, my_rows], 4, x_in)
+    to_mate(wu_hbm.at[:, there], wu_in.at[my_rows], 5, wu_in.at[pl.ds(0, width)])
+    to_mate(wd_hbm.at[there], wd_in.at[:, my_rows], 6, wd_in.at[:, pl.ds(0, width)])
+
+    arrived(0)
     part[c] = part[c] + swap_r[...].astype(F32)
     for j in range(nk):
         send_a[j] = part[c, j * seqs : (j + 1) * seqs, :].astype(BF16)
@@ -201,7 +215,7 @@
         peer = kv_peer(i)
         remote(send_a.at[peer], recv_a.at[me], 7, peer)
 
-    each(nk - 1, send_terms)
+    to_each(nk - 1, 7, recv_a, send_terms)
 
     row = lax.broadcasted_iota(jnp.int32, (seqs, size), 0)
     lane = lax.broadcasted_iota(jnp.int32, (seqs, size), 1)
@@ -214,12 +228,12 @@
     sine = jnp.where(lane < size // 2, -sine, sine)
     later[0].wait()
 
-    arrived(sq_r.at[pl.ds(0, nk - 1)], 1)
+    arrived(1)
     total_sq = jnp.sum(sq_r[...], axis=0)
     row_sq = jnp.sum(jnp.where(lane == row + me * seqs, total_sq, 0.0), axis=1, keepdims=True)
     scale1 = lax.rsqrt(row_sq / d_model + EPS)
 
-    arrived(recv_a.at[pl.ds(0, nk - 1)], 7)
+    arrived(7)
     queries, keys, values, gates = [], [], [], []
 
     def turn(v):
@@ -259,21 +273,21 @@
         peer = kv_peer(i)
         remote(ret_s.at[peer % 2], ret_r.at[me], 8, peer)
 
-    each(nk - 1, send_retained)
+    to_each(nk - 1, 8, ret_r, send_retained)
     state_copy = load(state_new, state_out, 11)
 
     later[1].wait()
     later[2].wait()
-    arrived(tok2.at[0], 2)
-    arrived(gain2.at[:, pl.ds(0, width)], 3)
-    arrived(wo_in.at[:, pl.ds(0, width)], 4)
+    arrived(2)
+    arrived(3)
+    arrived(4)
     for m in range(nb):
         for s in range(2):
             tok_rows[m, :, s * width : (s + 1) * width] = tok2[
                 s, m * per_chip : (m + 1) * per_chip
             ].astype(F32)
 
-    arrived(ret_r.at[pl.ds(0, nk - 1)], 8)
+    arrived(8)
     for j in range(nk):
         ret_f[j * seqs : (j + 1) * seqs] = ret_r[j].astype(F32)
     terms = jnp.dot(ret_f[...].astype(BF16), wo_in[...], preferred_element_type=F32)
@@ -285,10 +299,10 @@
             t, core = block_peer(i)
             remote(send_c.at[which, t * 2 + core], recv_c.at[which, block], phase, z * 2 + core, t)
 
-        each(nb - 1, send)
+        to_each(nb - 1, phase, recv_c.at[which], send)
 
     send_sums(0, 9)
-    arrived(recv_c.at[0, pl.ds(0, nb - 1)], 9)
+    arrived(9)
     mixed = (tok_rows[block] + jnp.sum(recv_c[0].astype(F32), axis=0)).astype(BF16)
     mix_s[...] = mixed
     mix_r[block] = mixed
@@ -297,10 +311,10 @@
         t, core = block_peer(i)
         remote(mix_s, mix_r.at[block], 10, z * 2 + core, t)
 
-    each(nb - 1, send_mixed)
+    to_each(nb - 1, 10, mix_r, send_mixed)
     later[3].wait()
-    arrived(wu_in.at[pl.ds(0, width)], 5)
-    arrived(mix_r.at[pl.ds(0, nb - 1)], 10)
+    arrived(5)
+    arrived(10)
     middle = mix_r[...].astype(F32).reshape(rows, 2 * width)
     square = middle * middle
     sq2_s[...] = jnp.sum(
@@ -311,7 +325,7 @@
     def send_squares2(i):
         remote(sq2_s, sq2_r.at[z], 11, chip_peer(i))
 
-    each(nz - 1, send_squares2)
+    to_each(nz - 1, 11, sq2_r, send_squares2)
     normed2 = (middle * gain2[...]).astype(BF16)
     upward = jnp.dot(normed2, wu_in[...], preferred_element_type=F32)
     send_d[...] = upward.reshape(nz, per_chip, half_ff).astype(BF16)
@@ -321,14 +335,14 @@
         peer = chip_peer(i)
         remote(send_d.at[peer // 2], recv_d.at[z], 12, peer)
 
-    each(nz - 1, send_up)
+    to_each(nz - 1, 12, recv_d, send_up)
     row = lax.broadcasted_iota(jnp.int32, (per_chip, size), 0)
     lane = lax.broadcasted_iota(jnp.int32, (per_chip, size), 1)
-    arrived(sq2_r.at[pl.ds(0, nz - 1)], 11)
+    arrived(11)
     total_sq = jnp.sum(sq2_r[...], axis=0)
     row_sq = jnp.sum(jnp.where(lane == row + z * per_chip, total_sq, 0.0), axis=1, keepdims=True)
     scale2 = lax.rsqrt(row_sq / d_model + EPS)
-    arrived(recv_d.at[pl.ds(0, nz - 1)], 12)
+    arrived(12)
     total = recv_d[0].astype(F32)
     for j in range(1, nz):
         total = total + recv_d[j].astype(F32)
@@ -339,16 +353,16 @@
     def send_hidden(i):
         remote(hid_s, hid_r.at[z], 13, chip_peer(i))
 
-    each(nz - 1, send_hidden)
+    to_each(nz - 1, 13, hid_r, send_hidden)
     later[4].wait()
-    arrived(wd_in.at[:, pl.ds(0, width)], 6)
-    arrived(hid_r.at[pl.ds(0, nz - 1)], 13)
+    arrived(6)
+    arrived(13)
     hidden_all = hid_r[...].astype(F32).reshape(rows, half_ff).astype(BF16)
     terms = jnp.dot(hidden_all, wd_in[...], preferred_element_type=F32)
     send_c[1] = terms.reshape(nb, per_chip, 2 * width).astype(BF16)
     recv_c[1, block] = send_c[1, block]
     send_sums(1, 14)
-    arrived(recv_c.at[1, pl.ds(0, nb - 1)], 14)
+    arrived(14)
     final = (mix_s[...].astype(F32) + jnp.sum(recv_c[1].astype(F32), axis=0)).astype(BF16)
     for s in range(2):
         out_s[s] = final[:, s * width : (s + 1) * width]
@@ -358,26 +372,10 @@
         t, core = block_peer(i)
         remote(out_s.at[core], out_r.at[block], 15, z * 2 + core, t)
 
-    each(nb - 1, send_out)
+    to_each(nb - 1, 15, out_r, send_out)
 
     state_copy.wait()
-    left(swap_s, 0)
-    left(sq_r.at[pl.ds(0, nk - 1)], 1)
-    left(x_in, 2)
-    left(gain_in, 3)
-    left(w_in.at[0, :, pl.ds(0, width)], 4)
-    left(wu_in.at[pl.ds(0, width)], 5)
-    left(wd_in.at[:, pl.ds(0, width)], 6)
-    left(send_a.at[pl.ds(0, nk - 1)], 7)
-    left(ret_r.at[pl.ds(0, nk - 1)], 8)
-    left(send_c.at[0, pl.ds(0, nb - 1)], 9)
-    left(mix_r.at[pl.ds(0, nb - 1)], 10)
-    left(sq2_r.at[pl.ds(0, nz - 1)], 11)
-    left(send_d.at[pl.ds(0, nz - 1)], 12)
-    left(hid_r.at[pl.ds(0, nz - 1)], 13)
-    left(send_c.at[1, pl.ds(0, nb - 1)], 14)
-    left(out_r.at[pl.ds(0, nb - 1)], 15)
-    arrived(out_r.at[pl.ds(0, nb - 1)], 15)
+    finish()
     out_ref[...] = out_r[...].astype(F32).reshape(rows, width).astype(BF16)
 
 
@@ -407,7 +405,7 @@
         inverse = 10000.0 ** (-(np.arange(size // 2, dtype=np.float64) * 2.0) / size)
         freq = jnp.asarray(np.concatenate([inverse, inverse])[None, :].astype(np.float32))
         cfg = (nk, nt, nz, width * nk, heads * nt)
-        anywhere = pl.BlockSpec(memory_space=pl.ANY)
+        anywhere = pl.BlockSpec(memory_space=pltpu.HBM)
         vmem = pl.BlockSpec(memory_space=pltpu.VMEM)
         smem = pl.BlockSpec(memory_space=pltpu.SMEM)
         scratch = [
@@ -460,7 +458,7 @@
                 pltpu.SemaphoreType.DMA((16,)),
             ],
             compiler_params=pltpu.CompilerParams(
-                collective_id=0, has_side_effects=True, vmem_limit_bytes=40 * 1024 * 1024
+                collective_id=0, has_side_effects=True
             ),
             name="step",
         )(

time: 127 us -> 121 us (0.953)
  local copies, waits for them, and re-layouts: 10.2 us -> 3.25 us
    unnamed x28 -> x2, local copies, waits for them, and re-layouts: 10.2 us -> 3.25 us
where the time goes in v2:
time: 121 us
  Pallas kernels  117 us (97%)
  local copies, waits for them, and re-layouts  3.25 us (3%)
    pallas_call x1, Pallas kernels, shards(): pl.pallas_call(functools.partial(kernel, cfg), out_shape=(jax.ShapeDtypeS...  117 us
    unnamed x2, local copies, waits for them, and re-layouts  3.25 us

profile of v2, /device:TPU:65, one launch (start us, length us, event | category | flops | bytes accessed | tf_op | source)
XLA Modules:
  0.0 120.7 jit_solution(17468544763361900332)
XLA Ops:
  0.6 116.8 %step.1 = (bf16[128,128]{1,0:T(8,128)(2,1)}, f32[4,2,128,128]{3,2,1,0:T(8,128)}) custom-call(s32[4]{0:T(128)} %pos_ref.1, bf16[128,128]{1,0:T(8,128)(2,1)} %x_hbm.1, f32[4,2,128,128]{3,2,1,0:T(8,128)} %state_hbm.1, f32[1,128]{1,0:T(1,128)} %bitcast.2, bf16[128,256]{1,0:T(8,128)(2,1)} %wq_hbm.1, bf16[128,256]{1,0:T(8,128)(2,1)} %wk_hbm.1, ...), custom_call_target="tpu_custom_call" | custom-call | tf_op jit(solution)/shard_map/step/pallas_call | solution.py:446
  117.4 1.4 %copy.17 = bf16[128,128]{1,0:T(8,128)(2,1)} copy(bf16[128,128]{1,0:T(8,128)(2,1)} %get-tuple-element.4) | data formatting | bytes 65536
  118.8 1.9 %copy.18 = f32[4,2,128,128]{3,2,1,0:T(8,128)} copy(f32[4,2,128,128]{3,2,1,0:T(8,128)} %get-tuple-element.5) | data formatting | bytes 1048576

commit v3 on v2

--- a/solution.py
+++ b/solution.py
@@ -21,7 +21,7 @@
 
 def kernel(
     cfg,
-    pos_ref,
+    pos_hbm,
     x_hbm,
     state_hbm,
     gain_hbm,
@@ -33,9 +33,11 @@
     gain2_hbm,
     wu_hbm,
     wd_hbm,
-    freq_ref,
+    freq_hbm,
     out_ref,
     state_out,
+    pos_ref,
+    freq_ref,
     x_in,
     gain_in,
     w_in,
@@ -64,6 +66,8 @@
     sq2_s,
     sq2_r,
     send_d,
+    near_d,
+    relay_d,
     recv_d,
     hid_s,
     hid_r,
@@ -72,8 +76,10 @@
     load_sem,
     send_sem,
     recv_sem,
+    near_sem,
+    far_sem,
 ):
-    nk, nt, nz, d_model, heads_all = cfg
+    nk, nt, nz, d_model, heads_all, relayed = cfg
     me = lax.axis_index("kv")
     tp = lax.axis_index("tp")
     z = me // 2
@@ -87,6 +93,7 @@
     per_chip = rows // nz
     size = width
     half_ff = wu_in.shape[1]
+    nr = near_d.shape[0]
 
     def kv_peer(step):
         chip = lax.rem(z + far_first(step // 2, nz), nz)
@@ -116,9 +123,6 @@
         pl.semaphore_signal(
             barrier, inc=1, device_id={"kv": z * 2 + core, "tp": t}, device_id_type=MESH
         )
-
-    each(nk - 1, greet_kv)
-    each(nb - 2, greet_block)
 
     def load(src, dst, sem):
         copy = pltpu.make_async_copy(src, dst, load_sem.at[sem])
@@ -132,7 +136,12 @@
         load(wk_hbm, w_in.at[1], 3),
         load(wv_hbm, w_in.at[2], 4),
         load(wg_hbm, w_in.at[3], 5),
+        load(pos_hbm, pos_ref, 12),
+        load(freq_hbm, freq_ref, 13),
     ]
+    each(nk - 1, greet_kv)
+    each(nb - 2, greet_block)
+
     here = pl.ds(pl.multiple_of(c * half_ff, 128), half_ff)
     there = pl.ds(pl.multiple_of((1 - c) * half_ff, 128), half_ff)
     mine = pl.ds(pl.multiple_of(c * size, 128), size)
@@ -329,34 +338,70 @@
     normed2 = (middle * gain2[...]).astype(BF16)
     upward = jnp.dot(normed2, wu_in[...], preferred_element_type=F32)
     send_d[...] = upward.reshape(nz, per_chip, half_ff).astype(BF16)
-    recv_d[z] = send_d[z]
-
-    def send_up(i):
-        peer = chip_peer(i)
-        remote(send_d.at[peer // 2], recv_d.at[z], 12, peer)
-
-    to_each(nz - 1, 12, recv_d, send_up)
+
+    def round_z(chip):
+        return chip - nz * (chip >= nz).astype(jnp.int32)
+
+    right, left = round_z(z + 1), round_z(z + nz - 1)
+
+    def near(src, dst, chip, at):
+        pltpu.make_async_remote_copy(
+            src_ref=src,
+            dst_ref=dst,
+            send_sem=send_sem.at[12],
+            recv_sem=near_sem.at[at],
+            device_id={"kv": chip * 2 + c},
+            device_id_type=MESH,
+        ).start()
+
+    def far(src, dst, chip, phase, at):
+        pltpu.make_async_remote_copy(
+            src_ref=src,
+            dst_ref=dst,
+            send_sem=send_sem.at[phase],
+            recv_sem=far_sem.at[at],
+            device_id={"kv": chip * 2 + c},
+            device_id_type=MESH,
+        ).start()
+
+    for k, offset in enumerate(relayed):
+        near(send_d.at[round_z(right + offset)], near_d.at[k, 0], right, k)
+        near(send_d.at[round_z(left + offset)], near_d.at[k, 1], left, k)
+    going[12] = send_d.at[pl.ds(0, 2 * nr)]
+    for k, offset in enumerate(relayed):
+        target = round_z(z + offset)
+        pltpu.make_async_copy(near_d.at[k], near_d.at[k], near_sem.at[k]).wait()
+        relay_d[k] = (
+            send_d[target].astype(F32) + near_d[k, 0].astype(F32) + near_d[k, 1].astype(F32)
+        ).astype(BF16)
+        far(relay_d.at[k], recv_d.at[k], target, 16, 0)
+    going[16] = relay_d
     row = lax.broadcasted_iota(jnp.int32, (per_chip, size), 0)
     lane = lax.broadcasted_iota(jnp.int32, (per_chip, size), 1)
     arrived(11)
     total_sq = jnp.sum(sq2_r[...], axis=0)
     row_sq = jnp.sum(jnp.where(lane == row + z * per_chip, total_sq, 0.0), axis=1, keepdims=True)
     scale2 = lax.rsqrt(row_sq / d_model + EPS)
-    arrived(12)
-    total = recv_d[0].astype(F32)
-    for j in range(1, nz):
-        total = total + recv_d[j].astype(F32)
+    pltpu.make_async_copy(recv_d, recv_d, far_sem.at[0]).wait()
+    total = send_d[z].astype(F32)
+    for k in range(nr):
+        total = total + recv_d[k].astype(F32)
     hidden = jnp.maximum(total * scale2, 0.0)
     hid_s[...] = (hidden * hidden).astype(BF16)
     hid_r[z] = hid_s[...]
 
-    def send_hidden(i):
-        remote(hid_s, hid_r.at[z], 13, chip_peer(i))
-
-    to_each(nz - 1, 13, hid_r, send_hidden)
+    for k, offset in enumerate(relayed):
+        far(hid_s, hid_r.at[z], round_z(z + offset), 13, k + 1)
+    going[13] = hid_r.at[pl.ds(0, nr)]
+    for k in reversed(range(nr)):
+        source = round_z(z + nz - relayed[k])
+        pltpu.make_async_copy(hid_r.at[source], hid_r.at[source], far_sem.at[k + 1]).wait()
+        for chip in (right, left):
+            remote(hid_r.at[source], hid_r.at[source], 17, chip * 2 + c)
+    going[17] = coming[17] = hid_r.at[pl.ds(0, 2 * nr)]
     later[4].wait()
     arrived(6)
-    arrived(13)
+    arrived(17)
     hidden_all = hid_r[...].astype(F32).reshape(rows, half_ff).astype(BF16)
     terms = jnp.dot(hidden_all, wd_in[...], preferred_element_type=F32)
     send_c[1] = terms.reshape(nb, per_chip, 2 * width).astype(BF16)
@@ -404,11 +449,13 @@
         nb = 2 * nt
         inverse = 10000.0 ** (-(np.arange(size // 2, dtype=np.float64) * 2.0) / size)
         freq = jnp.asarray(np.concatenate([inverse, inverse])[None, :].astype(np.float32))
-        cfg = (nk, nt, nz, width * nk, heads * nt)
         anywhere = pl.BlockSpec(memory_space=pltpu.HBM)
         vmem = pl.BlockSpec(memory_space=pltpu.VMEM)
-        smem = pl.BlockSpec(memory_space=pltpu.SMEM)
+        relayed = (8, 5, 11, 2, 14)
+        nr = len(relayed)
+        cfg = (nk, nt, nz, width * nk, heads * nt, relayed)
         scratch = [
+            ((1, size), F32),
             ((rows, width), BF16),
             ((1, width), F32),
             ((4, width, heads * size), BF16),
@@ -437,7 +484,9 @@
             ((1, rows), F32),
             ((nz, 1, rows), F32),
             ((nz, per_chip, ff // 2), BF16),
-            ((nz, per_chip, ff // 2), BF16),
+            ((nr, 2, per_chip, ff // 2), BF16),
+            ((nr, per_chip, ff // 2), BF16),
+            ((nr, per_chip, ff // 2), BF16),
             ((per_chip, ff // 2), BF16),
             ((nz, per_chip, ff // 2), BF16),
             ((2, per_chip, width), BF16),
@@ -449,13 +498,16 @@
                 jax.ShapeDtypeStruct((rows, width), BF16),
                 jax.ShapeDtypeStruct(state.shape, F32),
             ),
-            in_specs=[smem] + [anywhere] * 11 + [vmem],
+            in_specs=[anywhere] * 13,
             out_specs=(vmem, anywhere),
-            scratch_shapes=[pltpu.VMEM(s, t) for s, t in scratch]
+            scratch_shapes=[pltpu.SMEM((seqs,), jnp.int32)]
+            + [pltpu.VMEM(s, t) for s, t in scratch]
             + [
-                pltpu.SemaphoreType.DMA((12,)),
-                pltpu.SemaphoreType.DMA((16,)),
-                pltpu.SemaphoreType.DMA((16,)),
+                pltpu.SemaphoreType.DMA((14,)),
+                pltpu.SemaphoreType.DMA((18,)),
+                pltpu.SemaphoreType.DMA((18,)),
+                pltpu.SemaphoreType.DMA((nr,)),
+                pltpu.SemaphoreType.DMA((nr + 1,)),
             ],
             compiler_params=pltpu.CompilerParams(
                 collective_id=0, has_side_effects=True

time: 121 us -> 115 us (0.950)
  Pallas kernels: 117 us -> 111 us
    pallas_call x1, Pallas kernels: 117 us -> 111 us  [shards(): pl.pallas_call(functools.partial(kernel, cfg), out_shape=(jax.ShapeDtypeS...]
where the time goes in v3:
time: 115 us
  Pallas kernels  111 us (97%)
  local copies, waits for them, and re-layouts  3.25 us (3%)
    pallas_call x1, Pallas kernels, shards(): pl.pallas_call(functools.partial(kernel, cfg), out_shape=(jax.ShapeDtypeS...  111 us
    unnamed x2, local copies, waits for them, and re-layouts  3.25 us

profile of v3, /device:TPU:65, one launch (start us, length us, event | category | flops | bytes accessed | tf_op | source)
XLA Modules:
  0.0 115.0 jit_solution(12376178873752009701)
XLA Ops:
  0.6 111.1 %step.1 = (bf16[128,128]{1,0:T(8,128)(2,1)}, f32[4,2,128,128]{3,2,1,0:T(8,128)}) custom-call(s32[4]{0:T(128)} %pos_hbm.1, bf16[128,128]{1,0:T(8,128)(2,1)} %x_hbm.1, f32[4,2,128,128]{3,2,1,0:T(8,128)} %state_hbm.1, f32[1,128]{1,0:T(1,128)} %bitcast.2, bf16[128,256]{1,0:T(8,128)(2,1)} %wq_hbm.1, bf16[128,256]{1,0:T(8,128)(2,1)} %wk_hbm.1, ...), custom_call_target="tpu_custom_call" | custom-call | tf_op jit(solution)/shard_map/step/pallas_call | solution.py:495
  111.8 1.4 %copy.17 = bf16[128,128]{1,0:T(8,128)(2,1)} copy(bf16[128,128]{1,0:T(8,128)(2,1)} %get-tuple-element.4) | data formatting | bytes 65536
  113.1 1.9 %copy.18 = f32[4,2,128,128]{3,2,1,0:T(8,128)} copy(f32[4,2,128,128]{3,2,1,0:T(8,128)} %get-tuple-element.5) | data formatting | bytes 1048576

commit v4 on v3

--- a/solution.py
+++ b/solution.py
@@ -14,9 +14,8 @@
 EPS = 1e-06
 
 
-def far_first(step, count):
-    swing = (step + 1) // 2
-    return count // 2 + swing * (2 * (step % 2) - 1)
+def far_first(count):
+    return sorted(range(1, count), key=lambda offset: -min(offset, count - offset))
 
 
 def kernel(
@@ -52,6 +51,7 @@
     swap_s,
     swap_r,
     sq_s,
+    sq_m,
     sq_r,
     send_a,
     recv_a,
@@ -95,34 +95,15 @@
     half_ff = wu_in.shape[1]
     nr = near_d.shape[0]
 
-    def kv_peer(step):
-        chip = lax.rem(z + far_first(step // 2, nz), nz)
-        other = lax.rem(c + step % 2, 2)
-        last = (step == nk - 2).astype(jnp.int32)
-        return last * mate + (1 - last) * (chip * 2 + other)
-
-    def chip_peer(step):
-        return lax.rem(z + far_first(step, nz), nz) * 2 + c
-
-    def block_peer(step):
-        chip = lax.rem(tp + far_first(step // 2, nt), nt)
-        other = lax.rem(c + step % 2, 2)
-        last = (step == nb - 2).astype(jnp.int32)
-        return last * tp + (1 - last) * chip, last * (1 - c) + (1 - last) * other
-
-    def each(count, body):
-        lax.fori_loop(0, count, lambda i, carry: (body(i), carry)[1], 0)
+    def ring(at, count):
+        return at - count * (at >= count).astype(jnp.int32)
+
+    chips = [ring(z + offset, nz) for offset in far_first(nz)]
+    columns_x = [ring(tp + offset, nt) for offset in far_first(nt)]
+    kv_peers = [(chip * 2 + core, core) for chip in chips for core in range(2)] + [(mate, 1 - c)]
+    block_peers = [(t, core) for t in columns_x for core in range(2)] + [(tp, 1 - c)]
 
     barrier = pltpu.get_barrier_semaphore()
-
-    def greet_kv(i):
-        pl.semaphore_signal(barrier, inc=1, device_id={"kv": kv_peer(i)}, device_id_type=MESH)
-
-    def greet_block(i):
-        t, core = block_peer(i)
-        pl.semaphore_signal(
-            barrier, inc=1, device_id={"kv": z * 2 + core, "tp": t}, device_id_type=MESH
-        )
 
     def load(src, dst, sem):
         copy = pltpu.make_async_copy(src, dst, load_sem.at[sem])
@@ -139,8 +120,12 @@
         load(pos_hbm, pos_ref, 12),
         load(freq_hbm, freq_ref, 13),
     ]
-    each(nk - 1, greet_kv)
-    each(nb - 2, greet_block)
+    for peer, _ in kv_peers:
+        pl.semaphore_signal(barrier, inc=1, device_id={"kv": peer}, device_id_type=MESH)
+    for t, core in block_peers[:-1]:
+        pl.semaphore_signal(
+            barrier, inc=1, device_id={"kv": z * 2 + core, "tp": t}, device_id_type=MESH
+        )
 
     here = pl.ds(pl.multiple_of(c * half_ff, 128), half_ff)
     there = pl.ds(pl.multiple_of((1 - c) * half_ff, 128), half_ff)
@@ -161,7 +146,6 @@
     normed = (x * gain_in[...]).astype(BF16)
     square = x * x
     sq_s[...] = jnp.sum(jnp.transpose(square), axis=0, keepdims=True)
-    sq_r[me] = sq_s[...]
     for n in range(4):
         both = jnp.dot(normed, w_in[n], preferred_element_type=F32)
         part[0, :, n * size : (n + 1) * size] = both[:, :size]
@@ -188,8 +172,7 @@
         remote(src, dst, phase, mate)
         going[phase] = coming[phase] = amount
 
-    def to_each(count, phase, amount, send):
-        each(count, send)
+    def expect(count, phase, amount):
         going[phase] = coming[phase] = amount.at[pl.ds(0, count)]
 
     def arrived(phase):
@@ -204,27 +187,29 @@
 
     to_mate(swap_s, swap_r, 0, swap_r)
 
-    def send_squares(i):
-        remote(sq_s, sq_r.at[me], 1, kv_peer(i))
-
-    to_each(nk - 1, 1, sq_r, send_squares)
+    to_mate(sq_s, sq_m, 18, sq_m)
     to_mate(x_in, tok2.at[c], 2, x_in)
     to_mate(gain2_hbm, gain2.at[:, my_rows], 3, gain_in)
     to_mate(wo_hbm.at[other_head], wo_in.at[:, my_rows], 4, x_in)
     to_mate(wu_hbm.at[:, there], wu_in.at[my_rows], 5, wu_in.at[pl.ds(0, width)])
     to_mate(wd_hbm.at[there], wd_in.at[:, my_rows], 6, wd_in.at[:, pl.ds(0, width)])
 
+    arrived(18)
+    sq_r[z] = sq_s[...] + sq_m[...]
     arrived(0)
     part[c] = part[c] + swap_r[...].astype(F32)
     for j in range(nk):
         send_a[j] = part[c, j * seqs : (j + 1) * seqs, :].astype(BF16)
     recv_a[me] = send_a[me]
 
-    def send_terms(i):
-        peer = kv_peer(i)
-        remote(send_a.at[peer], recv_a.at[me], 7, peer)
-
-    to_each(nk - 1, 7, recv_a, send_terms)
+    for chip in chips:
+        for core in range(2):
+            peer = chip * 2 + core
+            remote(send_a.at[peer], recv_a.at[me], 7, peer)
+        remote(sq_r.at[z], sq_r.at[z], 1, chip * 2 + c)
+    remote(send_a.at[mate], recv_a.at[me], 7, mate)
+    expect(nk - 1, 7, recv_a)
+    expect(nz - 1, 1, sq_r)
 
     row = lax.broadcasted_iota(jnp.int32, (seqs, size), 0)
     lane = lax.broadcasted_iota(jnp.int32, (seqs, size), 1)
@@ -278,11 +263,9 @@
         ret_s[h] = (read * (gate / (1.0 + jnp.exp(-gate)))).astype(BF16)
     ret_r[me] = ret_s[c]
 
-    def send_retained(i):
-        peer = kv_peer(i)
-        remote(ret_s.at[peer % 2], ret_r.at[me], 8, peer)
-
-    to_each(nk - 1, 8, ret_r, send_retained)
+    for peer, core in kv_peers:
+        remote(ret_s.at[core], ret_r.at[me], 8, peer)
+    expect(nk - 1, 8, ret_r)
     state_copy = load(state_new, state_out, 11)
 
     later[1].wait()
@@ -304,11 +287,9 @@
     recv_c[0, block] = send_c[0, block]
 
     def send_sums(which, phase):
-        def send(i):
-            t, core = block_peer(i)
+        for t, core in block_peers:
             remote(send_c.at[which, t * 2 + core], recv_c.at[which, block], phase, z * 2 + core, t)
-
-        to_each(nb - 1, phase, recv_c.at[which], send)
+        expect(nb - 1, phase, recv_c.at[which])
 
     send_sums(0, 9)
     arrived(9)
@@ -316,11 +297,9 @@
     mix_s[...] = mixed
     mix_r[block] = mixed
 
-    def send_mixed(i):
-        t, core = block_peer(i)
+    for t, core in block_peers:
         remote(mix_s, mix_r.at[block], 10, z * 2 + core, t)
-
-    to_each(nb - 1, 10, mix_r, send_mixed)
+    expect(nb - 1, 10, mix_r)
     later[3].wait()
     arrived(5)
     arrived(10)
@@ -331,18 +310,14 @@
     )
     sq2_r[z] = sq2_s[...]
 
-    def send_squares2(i):
-        remote(sq2_s, sq2_r.at[z], 11, chip_peer(i))
-
-    to_each(nz - 1, 11, sq2_r, send_squares2)
+    for chip in chips:
+        remote(sq2_s, sq2_r.at[z], 11, chip * 2 + c)
+    expect(nz - 1, 11, sq2_r)
     normed2 = (middle * gain2[...]).astype(BF16)
     upward = jnp.dot(normed2, wu_in[...], preferred_element_type=F32)
     send_d[...] = upward.reshape(nz, per_chip, half_ff).astype(BF16)
 
-    def round_z(chip):
-        return chip - nz * (chip >= nz).astype(jnp.int32)
-
-    right, left = round_z(z + 1), round_z(z + nz - 1)
+    right, left = ring(z + 1, nz), ring(z + nz - 1, nz)
 
     def near(src, dst, chip, at):
         pltpu.make_async_remote_copy(
@@ -365,11 +340,11 @@
         ).start()
 
     for k, offset in enumerate(relayed):
-        near(send_d.at[round_z(right + offset)], near_d.at[k, 0], right, k)
-        near(send_d.at[round_z(left + offset)], near_d.at[k, 1], left, k)
+        near(send_d.at[ring(right + offset, nz)], near_d.at[k, 0], right, k)
+        near(send_d.at[ring(left + offset, nz)], near_d.at[k, 1], left, k)
     going[12] = send_d.at[pl.ds(0, 2 * nr)]
     for k, offset in enumerate(relayed):
-        target = round_z(z + offset)
+        target = ring(z + offset, nz)
         pltpu.make_async_copy(near_d.at[k], near_d.at[k], near_sem.at[k]).wait()
         relay_d[k] = (
             send_d[target].astype(F32) + near_d[k, 0].astype(F32) + near_d[k, 1].astype(F32)
@@ -391,10 +366,10 @@
     hid_r[z] = hid_s[...]
 
     for k, offset in enumerate(relayed):
-        far(hid_s, hid_r.at[z], round_z(z + offset), 13, k + 1)
+        far(hid_s, hid_r.at[z], ring(z + offset, nz), 13, k + 1)
     going[13] = hid_r.at[pl.ds(0, nr)]
     for k in reversed(range(nr)):
-        source = round_z(z + nz - relayed[k])
+        source = ring(z + nz - relayed[k], nz)
         pltpu.make_async_copy(hid_r.at[source], hid_r.at[source], far_sem.at[k + 1]).wait()
         for chip in (right, left):
             remote(hid_r.at[source], hid_r.at[source], 17, chip * 2 + c)
@@ -413,11 +388,9 @@
         out_s[s] = final[:, s * width : (s + 1) * width]
     out_r[block] = out_s[c]
 
-    def send_out(i):
-        t, core = block_peer(i)
+    for t, core in block_peers:
         remote(out_s.at[core], out_r.at[block], 15, z * 2 + core, t)
-
-    to_each(nb - 1, 15, out_r, send_out)
+    expect(nb - 1, 15, out_r)
 
     state_copy.wait()
     finish()
@@ -470,7 +443,8 @@
             ((rows, 4 * size), BF16),
             ((rows, 4 * size), BF16),
             ((1, rows), F32),
-            ((nk, 1, rows), F32),
+            ((1, rows), F32),
+            ((nz, 1, rows), F32),
             ((nk, seqs, 4 * size), BF16),
             ((nk, seqs, 4 * size), BF16),
             ((2, seqs, size), BF16),
@@ -504,8 +478,8 @@
             + [pltpu.VMEM(s, t) for s, t in scratch]
             + [
                 pltpu.SemaphoreType.DMA((14,)),
-                pltpu.SemaphoreType.DMA((18,)),
-                pltpu.SemaphoreType.DMA((18,)),
+                pltpu.SemaphoreType.DMA((19,)),
+                pltpu.SemaphoreType.DMA((19,)),
                 pltpu.SemaphoreType.DMA((nr,)),
                 pltpu.SemaphoreType.DMA((nr + 1,)),
             ],

time: 115 us -> 115 us (level)
  no operation moved by 1% of the time
where the time goes in v4:
time: 115 us
  Pallas kernels  111 us (97%)
  local copies, waits for them, and re-layouts  3.25 us (3%)
    pallas_call x1, Pallas kernels, shards(): pl.pallas_call(functools.partial(kernel, cfg), out_shape=(jax.ShapeDtypeS...  111 us
    unnamed x2, local copies, waits for them, and re-layouts  3.25 us

profile of v4, /device:TPU:65, one launch (start us, length us, event | category | flops | bytes accessed | tf_op | source)
XLA Modules:
  0.0 114.8 jit_solution(11737053581047541195)
XLA Ops:
  0.6 110.9 %step.1 = (bf16[128,128]{1,0:T(8,128)(2,1)}, f32[4,2,128,128]{3,2,1,0:T(8,128)}) custom-call(s32[4]{0:T(128)} %pos_hbm.1, bf16[128,128]{1,0:T(8,128)(2,1)} %x_hbm.1, f32[4,2,128,128]{3,2,1,0:T(8,128)} %state_hbm.1, f32[1,128]{1,0:T(1,128)} %bitcast.2, bf16[128,256]{1,0:T(8,128)(2,1)} %wq_hbm.1, bf16[128,256]{1,0:T(8,128)(2,1)} %wk_hbm.1, ...), custom_call_target="tpu_custom_call" | custom-call | tf_op jit(solution)/shard_map/step/pallas_call | solution.py:469
  111.5 1.4 %copy.17 = bf16[128,128]{1,0:T(8,128)(2,1)} copy(bf16[128,128]{1,0:T(8,128)(2,1)} %get-tuple-element.4) | data formatting | bytes 65536
  112.9 1.9 %copy.18 = f32[4,2,128,128]{3,2,1,0:T(8,128)} copy(f32[4,2,128,128]{3,2,1,0:T(8,128)} %get-tuple-element.5) | data formatting | bytes 1048576

commit v5 on v4

--- a/solution.py
+++ b/solution.py
@@ -70,6 +70,7 @@
     relay_d,
     recv_d,
     hid_s,
+    hid_in,
     hid_r,
     out_s,
     out_r,
@@ -319,38 +320,30 @@
 
     right, left = ring(z + 1, nz), ring(z + nz - 1, nz)
 
-    def near(src, dst, chip, at):
-        pltpu.make_async_remote_copy(
-            src_ref=src,
-            dst_ref=dst,
-            send_sem=send_sem.at[12],
-            recv_sem=near_sem.at[at],
-            device_id={"kv": chip * 2 + c},
-            device_id_type=MESH,
-        ).start()
-
-    def far(src, dst, chip, phase, at):
+    def hop(src, dst, kv, phase, sem):
         pltpu.make_async_remote_copy(
             src_ref=src,
             dst_ref=dst,
             send_sem=send_sem.at[phase],
-            recv_sem=far_sem.at[at],
-            device_id={"kv": chip * 2 + c},
+            recv_sem=sem,
+            device_id={"kv": kv},
             device_id_type=MESH,
         ).start()
 
     for k, offset in enumerate(relayed):
-        near(send_d.at[ring(right + offset, nz)], near_d.at[k, 0], right, k)
-        near(send_d.at[ring(left + offset, nz)], near_d.at[k, 1], left, k)
+        hop(send_d.at[ring(right + offset, nz)], near_d.at[k, 0], right * 2 + c, 12, near_sem.at[k])
+        hop(send_d.at[ring(left + offset, nz)], near_d.at[k, 1], left * 2 + c, 12, near_sem.at[k])
     going[12] = send_d.at[pl.ds(0, 2 * nr)]
+    hop(send_d.at[z], recv_d.at[nr], mate, 19, far_sem.at[0])
     for k, offset in enumerate(relayed):
         target = ring(z + offset, nz)
         pltpu.make_async_copy(near_d.at[k], near_d.at[k], near_sem.at[k]).wait()
         relay_d[k] = (
             send_d[target].astype(F32) + near_d[k, 0].astype(F32) + near_d[k, 1].astype(F32)
         ).astype(BF16)
-        far(relay_d.at[k], recv_d.at[k], target, 16, 0)
+        hop(relay_d.at[k], recv_d.at[k], target * 2 + 1 - c, 16, far_sem.at[0])
     going[16] = relay_d
+    going[19] = hid_s
     row = lax.broadcasted_iota(jnp.int32, (per_chip, size), 0)
     lane = lax.broadcasted_iota(jnp.int32, (per_chip, size), 1)
     arrived(11)
@@ -358,22 +351,21 @@
     row_sq = jnp.sum(jnp.where(lane == row + z * per_chip, total_sq, 0.0), axis=1, keepdims=True)
     scale2 = lax.rsqrt(row_sq / d_model + EPS)
     pltpu.make_async_copy(recv_d, recv_d, far_sem.at[0]).wait()
-    total = send_d[z].astype(F32)
-    for k in range(nr):
+    total = recv_d[0].astype(F32)
+    for k in range(1, nr + 1):
         total = total + recv_d[k].astype(F32)
     hidden = jnp.maximum(total * scale2, 0.0)
     hid_s[...] = (hidden * hidden).astype(BF16)
-    hid_r[z] = hid_s[...]
-
     for k, offset in enumerate(relayed):
-        far(hid_s, hid_r.at[z], ring(z + offset, nz), 13, k + 1)
-    going[13] = hid_r.at[pl.ds(0, nr)]
+        hop(hid_s, hid_in.at[k], ring(z + offset, nz) * 2 + c, 13, far_sem.at[k + 1])
+    going[13] = hid_in
+    remote(hid_s, hid_r.at[z], 17, mate)
     for k in reversed(range(nr)):
         source = ring(z + nz - relayed[k], nz)
-        pltpu.make_async_copy(hid_r.at[source], hid_r.at[source], far_sem.at[k + 1]).wait()
-        for chip in (right, left):
-            remote(hid_r.at[source], hid_r.at[source], 17, chip * 2 + c)
-    going[17] = coming[17] = hid_r.at[pl.ds(0, 2 * nr)]
+        pltpu.make_async_copy(hid_in.at[k], hid_in.at[k], far_sem.at[k + 1]).wait()
+        for kv in (right * 2 + 1 - c, left * 2 + 1 - c, mate):
+            remote(hid_in.at[k], hid_r.at[source], 17, kv)
+    going[17] = coming[17] = hid_r
     later[4].wait()
     arrived(6)
     arrived(17)
@@ -460,8 +452,9 @@
             ((nz, per_chip, ff // 2), BF16),
             ((nr, 2, per_chip, ff // 2), BF16),
             ((nr, per_chip, ff // 2), BF16),
+            ((nr + 1, per_chip, ff // 2), BF16),
+            ((per_chip, ff // 2), BF16),
             ((nr, per_chip, ff // 2), BF16),
-            ((per_chip, ff // 2), BF16),
             ((nz, per_chip, ff // 2), BF16),
             ((2, per_chip, width), BF16),
             ((nb, per_chip, width), BF16),
@@ -478,8 +471,8 @@
             + [pltpu.VMEM(s, t) for s, t in scratch]
             + [
                 pltpu.SemaphoreType.DMA((14,)),
-                pltpu.SemaphoreType.DMA((19,)),
-                pltpu.SemaphoreType.DMA((19,)),
+                pltpu.SemaphoreType.DMA((20,)),
+                pltpu.SemaphoreType.DMA((20,)),
                 pltpu.SemaphoreType.DMA((nr,)),
                 pltpu.SemaphoreType.DMA((nr + 1,)),
             ],

time: 115 us -> 113 us (0.983)
  Pallas kernels: 111 us -> 109 us
    pallas_call x1, Pallas kernels: 111 us -> 109 us  [shards(): pl.pallas_call(functools.partial(kernel, cfg), out_shape=(jax.ShapeDtypeS...]
where the time goes in v5:
time: 113 us
  Pallas kernels  109 us (96%)
  local copies, waits for them, and re-layouts  3.25 us (3%)
    pallas_call x1, Pallas kernels, shards(): pl.pallas_call(functools.partial(kernel, cfg), out_shape=(jax.ShapeDtypeS...  109 us
    unnamed x2, local copies, waits for them, and re-layouts  3.25 us

profile of v5, /device:TPU:65, one launch (start us, length us, event | category | flops | bytes accessed | tf_op | source)
XLA Modules:
  0.0 112.7 jit_solution(4058149635383197515)
XLA Ops:
  0.6 108.8 %step.1 = (bf16[128,128]{1,0:T(8,128)(2,1)}, f32[4,2,128,128]{3,2,1,0:T(8,128)}) custom-call(s32[4]{0:T(128)} %pos_hbm.1, bf16[128,128]{1,0:T(8,128)(2,1)} %x_hbm.1, f32[4,2,128,128]{3,2,1,0:T(8,128)} %state_hbm.1, f32[1,128]{1,0:T(1,128)} %bitcast.2, bf16[128,256]{1,0:T(8,128)(2,1)} %wq_hbm.1, bf16[128,256]{1,0:T(8,128)(2,1)} %wk_hbm.1, ...), custom_call_target="tpu_custom_call" | custom-call | tf_op jit(solution)/shard_map/step/pallas_call | solution.py:462
  109.4 1.4 %copy.17 = bf16[128,128]{1,0:T(8,128)(2,1)} copy(bf16[128,128]{1,0:T(8,128)(2,1)} %get-tuple-element.4) | data formatting | bytes 65536
  110.8 1.9 %copy.18 = f32[4,2,128,128]{3,2,1,0:T(8,128)} copy(f32[4,2,128,128]{3,2,1,0:T(8,128)} %get-tuple-element.5) | data formatting | bytes 1048576

commit v6 on v5

--- a/solution.py
+++ b/solution.py
@@ -86,8 +86,8 @@
     z = me // 2
     c = me % 2
     mate = me + 1 - 2 * c
-    block = tp * 2 + c
     nb = nt * 2
+    group = x_in.shape[0] // nt
     rows = x_in.shape[0]
     width = x_in.shape[1]
     seqs = rows // nk
@@ -177,14 +177,21 @@
         going[phase] = coming[phase] = amount.at[pl.ds(0, count)]
 
     def arrived(phase):
-        ref = coming.pop(phase)
-        pltpu.make_async_copy(ref, ref, recv_sem.at[phase]).wait()
+        pause(coming.pop(phase), recv_sem.at[phase])
+
+    def pause(amount, sem):
+        if isinstance(amount, tuple):
+            for core, one in enumerate(amount):
+                if one is not None:
+                    pl.when(c == core)(functools.partial(pause, one, sem))
+        else:
+            pltpu.make_async_copy(amount, amount, sem).wait()
 
     def finish():
         for phase in list(coming):
             arrived(phase)
-        for phase, ref in going.items():
-            pltpu.make_async_copy(ref, ref, send_sem.at[phase]).wait()
+        for phase, amount in going.items():
+            pause(amount, send_sem.at[phase])
 
     to_mate(swap_s, swap_r, 0, swap_r)
 
@@ -274,33 +281,51 @@
     arrived(2)
     arrived(3)
     arrived(4)
-    for m in range(nb):
+    for m in range(nt):
         for s in range(2):
             tok_rows[m, :, s * width : (s + 1) * width] = tok2[
-                s, m * per_chip : (m + 1) * per_chip
+                s, m * group : (m + 1) * group
             ].astype(F32)
 
     arrived(8)
     for j in range(nk):
         ret_f[j * seqs : (j + 1) * seqs] = ret_r[j].astype(F32)
     terms = jnp.dot(ret_f[...].astype(BF16), wo_in[...], preferred_element_type=F32)
-    send_c[0] = terms.reshape(nb, per_chip, 2 * width).astype(BF16)
-    recv_c[0, block] = send_c[0, block]
 
     def send_sums(which, phase):
-        for t, core in block_peers:
-            remote(send_c.at[which, t * 2 + core], recv_c.at[which, block], phase, z * 2 + core, t)
-        expect(nb - 1, phase, recv_c.at[which])
+        send_c[which] = terms.reshape(nt, group, 2 * width).astype(BF16)
+        slot = recv_c.at[which, tp * 2 + c]
+        for t in columns_x:
+            remote(send_c.at[which, t], slot, phase, z * 2 + 1, t)
+
+        @pl.when(c == 0)
+        def _():
+            remote(send_c.at[which, tp], slot, phase, mate)
+
+        @pl.when(c == 1)
+        def _():
+            recv_c[which, tp * 2 + 1] = send_c[which, tp]
+
+        going[phase] = (send_c.at[which], send_c.at[which, pl.ds(0, nt - 1)])
+        coming[phase] = (None, recv_c.at[which, pl.ds(0, nb - 1)])
+
+    def added(which):
+        return jnp.sum(recv_c[which].astype(F32), axis=0)
 
     send_sums(0, 9)
     arrived(9)
-    mixed = (tok_rows[block] + jnp.sum(recv_c[0].astype(F32), axis=0)).astype(BF16)
-    mix_s[...] = mixed
-    mix_r[block] = mixed
-
-    for t, core in block_peers:
-        remote(mix_s, mix_r.at[block], 10, z * 2 + core, t)
-    expect(nb - 1, 10, mix_r)
+    @pl.when(c == 1)
+    def _():
+        mixed = (tok_rows[tp] + added(0)).astype(BF16)
+        mix_s[...] = mixed
+        mix_r[tp] = mixed
+        for t in columns_x:
+            for core in range(2):
+                remote(mix_s, mix_r.at[tp], 10, z * 2 + core, t)
+        remote(mix_s, mix_r.at[tp], 10, mate)
+
+    going[10] = (None, recv_c.at[0, pl.ds(0, nb - 1)])
+    coming[10] = (mix_r, mix_r.at[pl.ds(0, nt - 1)])
     later[3].wait()
     arrived(5)
     arrived(10)
@@ -371,22 +396,25 @@
     arrived(17)
     hidden_all = hid_r[...].astype(F32).reshape(rows, half_ff).astype(BF16)
     terms = jnp.dot(hidden_all, wd_in[...], preferred_element_type=F32)
-    send_c[1] = terms.reshape(nb, per_chip, 2 * width).astype(BF16)
-    recv_c[1, block] = send_c[1, block]
     send_sums(1, 14)
     arrived(14)
-    final = (mix_s[...].astype(F32) + jnp.sum(recv_c[1].astype(F32), axis=0)).astype(BF16)
-    for s in range(2):
-        out_s[s] = final[:, s * width : (s + 1) * width]
-    out_r[block] = out_s[c]
-
-    for t, core in block_peers:
-        remote(out_s.at[core], out_r.at[block], 15, z * 2 + core, t)
-    expect(nb - 1, 15, out_r)
+    @pl.when(c == 1)
+    def _():
+        final = (mix_s[...].astype(F32) + added(1)).astype(BF16)
+        for s in range(2):
+            out_s[s] = final[:, s * width : (s + 1) * width]
+        out_r[tp] = out_s[1]
+        for t in columns_x:
+            for core in range(2):
+                remote(out_s.at[core], out_r.at[tp], 15, z * 2 + core, t)
+        remote(out_s.at[0], out_r.at[tp], 15, mate)
+
+    going[15] = (None, recv_c.at[0, pl.ds(0, nb - 1), :, pl.ds(0, width)])
+    coming[15] = (out_r, out_r.at[pl.ds(0, nt - 1)])
 
     state_copy.wait()
     finish()
-    out_ref[...] = out_r[...].astype(F32).reshape(rows, width).astype(BF16)
+    out_ref[...] = out_r[...].reshape(rows, width)
 
 
 def solution(mesh):
@@ -412,6 +440,7 @@
         ff = w_up.shape[1]
         per_chip = rows // nz
         nb = 2 * nt
+        group = rows // nt
         inverse = 10000.0 ** (-(np.arange(size // 2, dtype=np.float64) * 2.0) / size)
         freq = jnp.asarray(np.concatenate([inverse, inverse])[None, :].astype(np.float32))
         anywhere = pl.BlockSpec(memory_space=pltpu.HBM)
@@ -442,11 +471,11 @@
             ((2, seqs, size), BF16),
             ((nk, seqs, size), BF16),
             ((rows, size), F32),
-            ((2, nb, per_chip, 2 * width), BF16),
-            ((2, nb, per_chip, 2 * width), BF16),
-            ((nb, per_chip, 2 * width), F32),
-            ((per_chip, 2 * width), BF16),
-            ((nb, per_chip, 2 * width), BF16),
+            ((2, nt, group, 2 * width), BF16),
+            ((2, nb, group, 2 * width), BF16),
+            ((nt, group, 2 * width), F32),
+            ((group, 2 * width), BF16),
+            ((nt, group, 2 * width), BF16),
             ((1, rows), F32),
             ((nz, 1, rows), F32),
             ((nz, per_chip, ff // 2), BF16),
@@ -456,8 +485,8 @@
             ((per_chip, ff // 2), BF16),
             ((nr, per_chip, ff // 2), BF16),
             ((nz, per_chip, ff // 2), BF16),
-            ((2, per_chip, width), BF16),
-            ((nb, per_chip, width), BF16),
+            ((2, group, width), BF16),
+            ((nt, group, width), BF16),
         ]
         return pl.pallas_call(
             functools.partial(kernel, cfg),

time: 113 us -> 112 us (level)
  no operation moved by 1% of the time
where the time goes in v6:
time: 112 us
  Pallas kernels  108 us (96%)
  local copies, waits for them, and re-layouts  3.25 us (3%)
    pallas_call x1, Pallas kernels, shards(): pl.pallas_call(functools.partial(kernel, cfg), out_shape=(jax.ShapeDtypeS...  108 us
    unnamed x2, local copies, waits for them, and re-layouts  3.25 us

profile of v6, /device:TPU:65, one launch (start us, length us, event | category | flops | bytes accessed | tf_op | source)
XLA Modules:
  0.0 111.9 jit_solution(16761003584596543226)
XLA Ops:
  0.6 108.1 %step.1 = (bf16[128,128]{1,0:T(8,128)(2,1)}, f32[4,2,128,128]{3,2,1,0:T(8,128)}) custom-call(s32[4]{0:T(128)} %pos_hbm.1, bf16[128,128]{1,0:T(8,128)(2,1)} %x_hbm.1, f32[4,2,128,128]{3,2,1,0:T(8,128)} %state_hbm.1, f32[1,128]{1,0:T(1,128)} %bitcast.2, bf16[128,256]{1,0:T(8,128)(2,1)} %wq_hbm.1, bf16[128,256]{1,0:T(8,128)(2,1)} %wk_hbm.1, ...), custom_call_target="tpu_custom_call" | custom-call | tf_op jit(solution)/shard_map/step/pallas_call | solution.py:491
  108.7 1.4 %copy.17 = bf16[128,128]{1,0:T(8,128)(2,1)} copy(bf16[128,128]{1,0:T(8,128)(2,1)} %get-tuple-element.4) | data formatting | bytes 65536
  110.1 1.9 %copy.18 = f32[4,2,128,128]{3,2,1,0:T(8,128)} copy(f32[4,2,128,128]{3,2,1,0:T(8,128)} %get-tuple-element.5) | data formatting | bytes 1048576

commit v7 on v6

--- a/solution.py
+++ b/solution.py
@@ -66,8 +66,6 @@
     sq2_s,
     sq2_r,
     send_d,
-    near_d,
-    relay_d,
     recv_d,
     hid_s,
     hid_in,
@@ -77,7 +75,6 @@
     load_sem,
     send_sem,
     recv_sem,
-    near_sem,
     far_sem,
 ):
     nk, nt, nz, d_model, heads_all, relayed = cfg
@@ -93,8 +90,13 @@
     seqs = rows // nk
     per_chip = rows // nz
     size = width
-    half_ff = wu_in.shape[1]
-    nr = near_d.shape[0]
+    half_ff = wd_in.shape[0]
+    quarter = wu_in.shape[1]
+    pair = z // 2
+    b = z % 2
+    beside = z + 1 - 2 * b
+    half_nz = nz // 2
+    nr = hid_in.shape[0]
 
     def ring(at, count):
         return at - count * (at >= count).astype(jnp.int32)
@@ -102,7 +104,7 @@
     chips = [ring(z + offset, nz) for offset in far_first(nz)]
     columns_x = [ring(tp + offset, nt) for offset in far_first(nt)]
     kv_peers = [(chip * 2 + core, core) for chip in chips for core in range(2)] + [(mate, 1 - c)]
-    block_peers = [(t, core) for t in columns_x for core in range(2)] + [(tp, 1 - c)]
+    pairs = [ring(pair + offset, half_nz) for offset in far_first(half_nz)]
 
     barrier = pltpu.get_barrier_semaphore()
 
@@ -123,21 +125,28 @@
     ]
     for peer, _ in kv_peers:
         pl.semaphore_signal(barrier, inc=1, device_id={"kv": peer}, device_id_type=MESH)
-    for t, core in block_peers[:-1]:
-        pl.semaphore_signal(
-            barrier, inc=1, device_id={"kv": z * 2 + core, "tp": t}, device_id_type=MESH
-        )
+    for t in columns_x:
+        for chip in (z, beside):
+            for core in range(2):
+                pl.semaphore_signal(
+                    barrier, inc=1, device_id={"kv": chip * 2 + core, "tp": t}, device_id_type=MESH
+                )
 
     here = pl.ds(pl.multiple_of(c * half_ff, 128), half_ff)
     there = pl.ds(pl.multiple_of((1 - c) * half_ff, 128), half_ff)
     mine = pl.ds(pl.multiple_of(c * size, 128), size)
     other_head = pl.ds(pl.multiple_of((1 - c) * size, 128), size)
     my_rows = pl.ds(pl.multiple_of(c * width, 128), width)
+    my_place = pl.ds(pl.multiple_of((b * 2 + c) * width, 128), width)
+
+    def up_part(half, core):
+        return pl.ds(pl.multiple_of(core * half_ff + half * quarter, 128), quarter)
+
     later = [
         load(state_hbm, state_in, 6),
         load(wo_hbm.at[mine], wo_in.at[:, my_rows], 7),
-        load(gain2_hbm, gain2.at[:, my_rows], 8),
-        load(wu_hbm.at[:, here], wu_in.at[my_rows], 9),
+        load(gain2_hbm, gain2.at[:, my_place], 8),
+        load(wu_hbm.at[:, up_part(b, c)], wu_in.at[my_place], 9),
         load(wd_hbm.at[here], wd_in.at[:, my_rows], 10),
     ]
 
@@ -154,7 +163,7 @@
     swap_s[...] = part[1 - c].astype(BF16)
     tok2[c] = x_in[...]
 
-    pl.semaphore_wait(barrier, nk - 1 + nb - 2)
+    pl.semaphore_wait(barrier, nk - 1 + 4 * (nt - 1))
 
     going, coming = {}, {}
 
@@ -197,9 +206,7 @@
 
     to_mate(sq_s, sq_m, 18, sq_m)
     to_mate(x_in, tok2.at[c], 2, x_in)
-    to_mate(gain2_hbm, gain2.at[:, my_rows], 3, gain_in)
     to_mate(wo_hbm.at[other_head], wo_in.at[:, my_rows], 4, x_in)
-    to_mate(wu_hbm.at[:, there], wu_in.at[my_rows], 5, wu_in.at[pl.ds(0, width)])
     to_mate(wd_hbm.at[there], wd_in.at[:, my_rows], 6, wd_in.at[:, pl.ds(0, width)])
 
     arrived(18)
@@ -274,6 +281,12 @@
     for peer, core in kv_peers:
         remote(ret_s.at[core], ret_r.at[me], 8, peer)
     expect(nk - 1, 8, ret_r)
+    for half, core in ((b, 1 - c), (1 - b, 0), (1 - b, 1)):
+        kv = (pair * 2 + half) * 2 + core
+        remote(gain2_hbm, gain2.at[:, my_place], 3, kv)
+        remote(wu_hbm.at[:, up_part(half, core)], wu_in.at[my_place], 5, kv)
+    going[3] = coming[3] = gain2.at[:, pl.ds(0, 3 * width)]
+    going[5] = coming[5] = wu_in.at[pl.ds(0, 3 * width)]
     state_copy = load(state_new, state_out, 11)
 
     later[1].wait()
@@ -318,32 +331,36 @@
     def _():
         mixed = (tok_rows[tp] + added(0)).astype(BF16)
         mix_s[...] = mixed
-        mix_r[tp] = mixed
+        mix_r[b, tp] = mixed
         for t in columns_x:
             for core in range(2):
-                remote(mix_s, mix_r.at[tp], 10, z * 2 + core, t)
-        remote(mix_s, mix_r.at[tp], 10, mate)
+                remote(mix_s, mix_r.at[b, tp], 20, beside * 2 + core, t)
+                remote(mix_s, mix_r.at[b, tp], 10, z * 2 + core, t)
+        for core in range(2):
+            remote(mix_s, mix_r.at[b, tp], 20, beside * 2 + core)
+        remote(mix_s, mix_r.at[b, tp], 10, mate)
 
     going[10] = (None, recv_c.at[0, pl.ds(0, nb - 1)])
-    coming[10] = (mix_r, mix_r.at[pl.ds(0, nt - 1)])
+    going[20] = (None, recv_c.at[0])
+    coming[10] = (mix_r.at[0], mix_r.at[0, pl.ds(0, nt - 1)])
+    coming[20] = mix_r.at[0]
     later[3].wait()
     arrived(5)
     arrived(10)
-    middle = mix_r[...].astype(F32).reshape(rows, 2 * width)
+    arrived(20)
+    middle = jnp.concatenate(
+        [mix_r[half].astype(F32).reshape(rows, 2 * width) for half in range(2)], axis=1
+    )
     square = middle * middle
-    sq2_s[...] = jnp.sum(
-        jnp.transpose(square[:, :width] + square[:, width:]), axis=0, keepdims=True
-    )
-    sq2_r[z] = sq2_s[...]
-
-    for chip in chips:
-        remote(sq2_s, sq2_r.at[z], 11, chip * 2 + c)
-    expect(nz - 1, 11, sq2_r)
+    square = sum(square[:, k * width : (k + 1) * width] for k in range(4))
+    sq2_s[...] = jnp.sum(jnp.transpose(square), axis=0, keepdims=True)
+    sq2_r[pair] = sq2_s[...]
+    for other in pairs:
+        remote(sq2_s, sq2_r.at[pair], 11, (other * 2 + b) * 2 + 1 - c)
+    expect(half_nz - 1, 11, sq2_r)
     normed2 = (middle * gain2[...]).astype(BF16)
     upward = jnp.dot(normed2, wu_in[...], preferred_element_type=F32)
-    send_d[...] = upward.reshape(nz, per_chip, half_ff).astype(BF16)
-
-    right, left = ring(z + 1, nz), ring(z + nz - 1, nz)
+    send_d[...] = upward.reshape(half_nz, 2 * per_chip, quarter).astype(BF16)
 
     def hop(src, dst, kv, phase, sem):
         pltpu.make_async_remote_copy(
@@ -355,47 +372,45 @@
             device_id_type=MESH,
         ).start()
 
-    for k, offset in enumerate(relayed):
-        hop(send_d.at[ring(right + offset, nz)], near_d.at[k, 0], right * 2 + c, 12, near_sem.at[k])
-        hop(send_d.at[ring(left + offset, nz)], near_d.at[k, 1], left * 2 + c, 12, near_sem.at[k])
-    going[12] = send_d.at[pl.ds(0, 2 * nr)]
-    hop(send_d.at[z], recv_d.at[nr], mate, 19, far_sem.at[0])
-    for k, offset in enumerate(relayed):
-        target = ring(z + offset, nz)
-        pltpu.make_async_copy(near_d.at[k], near_d.at[k], near_sem.at[k]).wait()
-        relay_d[k] = (
-            send_d[target].astype(F32) + near_d[k, 0].astype(F32) + near_d[k, 1].astype(F32)
-        ).astype(BF16)
-        hop(relay_d.at[k], recv_d.at[k], target * 2 + 1 - c, 16, far_sem.at[0])
-    going[16] = relay_d
-    going[19] = hid_s
-    row = lax.broadcasted_iota(jnp.int32, (per_chip, size), 0)
-    lane = lax.broadcasted_iota(jnp.int32, (per_chip, size), 1)
+    for other in pairs:
+        remote(send_d.at[other], recv_d.at[pair], 12, (other * 2 + b) * 2 + 1 - c)
+    remote(send_d.at[pair], recv_d.at[pair], 12, mate)
+    going[12] = coming[12] = recv_d
+    right, left = ring(z + 1, nz), ring(z + nz - 1, nz)
+    row = lax.broadcasted_iota(jnp.int32, (2 * per_chip, size), 0)
+    lane = lax.broadcasted_iota(jnp.int32, (2 * per_chip, size), 1)
     arrived(11)
     total_sq = jnp.sum(sq2_r[...], axis=0)
-    row_sq = jnp.sum(jnp.where(lane == row + z * per_chip, total_sq, 0.0), axis=1, keepdims=True)
+    row_sq = jnp.sum(jnp.where(lane == row + pair * 2 * per_chip, total_sq, 0.0), axis=1, keepdims=True)
     scale2 = lax.rsqrt(row_sq / d_model + EPS)
-    pltpu.make_async_copy(recv_d, recv_d, far_sem.at[0]).wait()
+    arrived(12)
     total = recv_d[0].astype(F32)
-    for k in range(1, nr + 1):
+    for k in range(1, half_nz):
         total = total + recv_d[k].astype(F32)
     hidden = jnp.maximum(total * scale2, 0.0)
     hid_s[...] = (hidden * hidden).astype(BF16)
     for k, offset in enumerate(relayed):
-        hop(hid_s, hid_in.at[k], ring(z + offset, nz) * 2 + c, 13, far_sem.at[k + 1])
+        hop(hid_s, hid_in.at[k], ring(z + offset, nz) * 2 + c, 13, far_sem.at[k])
     going[13] = hid_in
     remote(hid_s, hid_r.at[z], 17, mate)
     for k in reversed(range(nr)):
         source = ring(z + nz - relayed[k], nz)
-        pltpu.make_async_copy(hid_in.at[k], hid_in.at[k], far_sem.at[k + 1]).wait()
+        pltpu.make_async_copy(hid_in.at[k], hid_in.at[k], far_sem.at[k]).wait()
         for kv in (right * 2 + 1 - c, left * 2 + 1 - c, mate):
             remote(hid_in.at[k], hid_r.at[source], 17, kv)
     going[17] = coming[17] = hid_r
     later[4].wait()
     arrived(6)
     arrived(17)
-    hidden_all = hid_r[...].astype(F32).reshape(rows, half_ff).astype(BF16)
-    terms = jnp.dot(hidden_all, wd_in[...], preferred_element_type=F32)
+    everyone = hid_r[...].reshape(half_nz, 2, 2 * per_chip, quarter)
+    terms = sum(
+        jnp.dot(
+            everyone[:, half].reshape(rows, quarter),
+            wd_in[half * quarter : (half + 1) * quarter],
+            preferred_element_type=F32,
+        )
+        for half in range(2)
+    )
     send_sums(1, 14)
     arrived(14)
     @pl.when(c == 1)
@@ -456,10 +471,10 @@
             (state.shape, F32),
             (state.shape, F32),
             ((size, 2 * width), BF16),
-            ((2 * width, ff // 2), BF16),
+            ((4 * width, ff // 4), BF16),
             ((ff // 2, 2 * width), BF16),
             ((2, rows, width), BF16),
-            ((1, 2 * width), F32),
+            ((1, 4 * width), F32),
             ((2, rows, 4 * size), F32),
             ((rows, 4 * size), BF16),
             ((rows, 4 * size), BF16),
@@ -475,16 +490,14 @@
             ((2, nb, group, 2 * width), BF16),
             ((nt, group, 2 * width), F32),
             ((group, 2 * width), BF16),
-            ((nt, group, 2 * width), BF16),
+            ((2, nt, group, 2 * width), BF16),
             ((1, rows), F32),
-            ((nz, 1, rows), F32),
-            ((nz, per_chip, ff // 2), BF16),
-            ((nr, 2, per_chip, ff // 2), BF16),
-            ((nr, per_chip, ff // 2), BF16),
-            ((nr + 1, per_chip, ff // 2), BF16),
-            ((per_chip, ff // 2), BF16),
-            ((nr, per_chip, ff // 2), BF16),
-            ((nz, per_chip, ff // 2), BF16),
+            ((nz // 2, 1, rows), F32),
+            ((nz // 2, 2 * per_chip, ff // 4), BF16),
+            ((nz // 2, 2 * per_chip, ff // 4), BF16),
+            ((2 * per_chip, ff // 4), BF16),
+            ((nr, 2 * per_chip, ff // 4), BF16),
+            ((nz, 2 * per_chip, ff // 4), BF16),
             ((2, group, width), BF16),
             ((nt, group, width), BF16),
         ]
@@ -500,10 +513,9 @@
             + [pltpu.VMEM(s, t) for s, t in scratch]
             + [
                 pltpu.SemaphoreType.DMA((14,)),
-                pltpu.SemaphoreType.DMA((20,)),
-                pltpu.SemaphoreType.DMA((20,)),
+                pltpu.SemaphoreType.DMA((21,)),
+                pltpu.SemaphoreType.DMA((21,)),
                 pltpu.SemaphoreType.DMA((nr,)),
-                pltpu.SemaphoreType.DMA((nr + 1,)),
             ],
             compiler_params=pltpu.CompilerParams(
                 collective_id=0, has_side_effects=True

time: 112 us -> 113 us (level)
    pallas_call x1, Pallas kernels: 108 us -> 109 us  [shards(): pl.pallas_call(functools.partial(kernel, cfg), out_shape=(jax.ShapeDtypeS...]
where the time goes in v7:
time: 113 us
  Pallas kernels  109 us (96%)
  local copies, waits for them, and re-layouts  3.25 us (3%)
    pallas_call x1, Pallas kernels, shards(): pl.pallas_call(functools.partial(kernel, cfg), out_shape=(jax.ShapeDtypeS...  109 us
    unnamed x2, local copies, waits for them, and re-layouts  3.25 us

profile of v7, /device:TPU:65, one launch (start us, length us, event | category | flops | bytes accessed | tf_op | source)
XLA Modules:
  0.0 113.2 jit_solution(15575537101719732947)
XLA Ops:
  0.6 109.3 %step.1 = (bf16[128,128]{1,0:T(8,128)(2,1)}, f32[4,2,128,128]{3,2,1,0:T(8,128)}) custom-call(s32[4]{0:T(128)} %pos_hbm.1, bf16[128,128]{1,0:T(8,128)(2,1)} %x_hbm.1, f32[4,2,128,128]{3,2,1,0:T(8,128)} %state_hbm.1, f32[1,128]{1,0:T(1,128)} %bitcast.2, bf16[128,256]{1,0:T(8,128)(2,1)} %wq_hbm.1, bf16[128,256]{1,0:T(8,128)(2,1)} %wk_hbm.1, ...), custom_call_target="tpu_custom_call" | custom-call | tf_op jit(solution)/shard_map/step/pallas_call | solution.py:504
  110.0 1.4 %copy.17 = bf16[128,128]{1,0:T(8,128)(2,1)} copy(bf16[128,128]{1,0:T(8,128)(2,1)} %get-tuple-element.4) | data formatting | bytes 65536
  111.3 1.9 %copy.18 = f32[4,2,128,128]{3,2,1,0:T(8,128)} copy(f32[4,2,128,128]{3,2,1,0:T(8,128)} %get-tuple-element.5) | data formatting | bytes 1048576

commit v8 on v6

--- a/solution.py
+++ b/solution.py
@@ -41,7 +41,6 @@
     gain_in,
     w_in,
     state_in,
-    state_new,
     wo_in,
     wu_in,
     wd_in,
@@ -263,7 +262,7 @@
                 gamma * state_in[i, h]
                 + columns[:, 2 * seqs + at : 2 * seqs + at + 1] * values[h][i : i + 1]
             )
-            state_new[i, h] = new
+            state_out[i, h] = new
             reads.append(jnp.sum(columns[:, at : at + 1] * new, axis=0, keepdims=True))
         read = jnp.concatenate(reads, axis=0)
         read = read * lax.rsqrt(jnp.mean(read * read, axis=1, keepdims=True) + EPS)
@@ -274,7 +273,6 @@
     for peer, core in kv_peers:
         remote(ret_s.at[core], ret_r.at[me], 8, peer)
     expect(nk - 1, 8, ret_r)
-    state_copy = load(state_new, state_out, 11)
 
     later[1].wait()
     later[2].wait()
@@ -412,7 +410,6 @@
     going[15] = (None, recv_c.at[0, pl.ds(0, nb - 1), :, pl.ds(0, width)])
     coming[15] = (out_r, out_r.at[pl.ds(0, nt - 1)])
 
-    state_copy.wait()
     finish()
     out_ref[...] = out_r[...].reshape(rows, width)
 
@@ -453,7 +450,6 @@
             ((rows, width), BF16),
             ((1, width), F32),
             ((4, width, heads * size), BF16),
-            (state.shape, F32),
             (state.shape, F32),
             ((size, 2 * width), BF16),
             ((2 * width, ff // 2), BF16),
@@ -491,11 +487,11 @@
         return pl.pallas_call(
             functools.partial(kernel, cfg),
             out_shape=(
-                jax.ShapeDtypeStruct((rows, width), BF16),
-                jax.ShapeDtypeStruct(state.shape, F32),
+                pltpu.VMEM((rows, width), BF16),
+                pltpu.VMEM(state.shape, F32),
             ),
             in_specs=[anywhere] * 13,
-            out_specs=(vmem, anywhere),
+            out_specs=(vmem, vmem),
             scratch_shapes=[pltpu.SMEM((seqs,), jnp.int32)]
             + [pltpu.VMEM(s, t) for s, t in scratch]
             + [

time: 112 us -> 110 us (0.982)
  local copies, waits for them, and re-layouts: 3.25 us -> 1.41 us
    unnamed x2, local copies, waits for them, and re-layouts: 3.25 us -> 1.41 us
where the time goes in v8:
time: 110 us
  Pallas kernels  107 us (97%)
  local copies, waits for them, and re-layouts  1.41 us (1%)
    pallas_call x1, Pallas kernels, shards(): pl.pallas_call(functools.partial(kernel, cfg), out_shape=(pltpu.VMEM((row...  107 us

profile of v8, /device:TPU:65, one launch (start us, length us, event | category | flops | bytes accessed | tf_op | source)
XLA Modules:
  0.0 109.5 jit_solution(13072800215527259396)
XLA Ops:
  0.6 107.4 %step.1 = (bf16[128,128]{1,0:T(8,128)(2,1)S(1)}, f32[4,2,128,128]{3,2,1,0:T(8,128)S(1)}) custom-call(s32[4]{0:T(128)} %pos_hbm.1, bf16[128,128]{1,0:T(8,128)(2,1)} %x_hbm.1, f32[4,2,128,128]{3,2,1,0:T(8,128)} %state_hbm.1, f32[1,128]{1,0:T(1,128)} %bitcast.2, bf16[128,256]{1,0:T(8,128)(2,1)} %wq_hbm.1, bf16[128,256]{1,0:T(8,128)(2,1)} %wk_hbm.1, ...), custom_call_target="tpu_custom_call" | custom-call | tf_op jit(solution)/shard_map/step/pallas_call | solution.py:487
  108.1 0.6 copy.17
  108.7 0.8 copy.18

commit v9 on v8

--- a/solution.py
+++ b/solution.py
@@ -54,6 +54,9 @@
     sq_r,
     send_a,
     recv_a,
+    send_u,
+    recv_u,
+    sq_u,
     ret_s,
     ret_r,
     ret_f,
@@ -99,6 +102,7 @@
         return at - count * (at >= count).astype(jnp.int32)
 
     chips = [ring(z + offset, nz) for offset in far_first(nz)]
+    nu = recv_u.shape[0]
     columns_x = [ring(tp + offset, nt) for offset in far_first(nt)]
     kv_peers = [(chip * 2 + core, core) for chip in chips for core in range(2)] + [(mate, 1 - c)]
     block_peers = [(t, core) for t in columns_x for core in range(2)] + [(tp, 1 - c)]
@@ -110,6 +114,11 @@
         copy.start()
         return copy
 
+    def greet(peers):
+        for peer, _ in peers:
+            pl.semaphore_signal(barrier, inc=1, device_id={"kv": peer}, device_id_type=MESH)
+
+    greet(kv_peers[: 2 * nu])
     first = [
         load(x_hbm, x_in, 0),
         load(gain_hbm, gain_in, 1),
@@ -120,8 +129,7 @@
         load(pos_hbm, pos_ref, 12),
         load(freq_hbm, freq_ref, 13),
     ]
-    for peer, _ in kv_peers:
-        pl.semaphore_signal(barrier, inc=1, device_id={"kv": peer}, device_id_type=MESH)
+    greet(kv_peers[2 * nu :])
     for t, core in block_peers[:-1]:
         pl.semaphore_signal(
             barrier, inc=1, device_id={"kv": z * 2 + core, "tp": t}, device_id_type=MESH
@@ -152,6 +160,14 @@
         part[1, :, n * size : (n + 1) * size] = both[:, size:]
     swap_s[...] = part[1 - c].astype(BF16)
     tok2[c] = x_in[...]
+    for j in range(nk):
+        for h in range(2):
+            send_u[j, h] = part[h, j * seqs : (j + 1) * seqs, :].astype(BF16)
+    for offset in far_first(nz)[:nu]:
+        source = ring(z + nz - offset, nz)
+        sq_r[source] = jnp.zeros_like(sq_s)
+        for core in range(2):
+            recv_a[source * 2 + core] = jnp.zeros(recv_a.shape[1:], BF16)
 
     pl.semaphore_wait(barrier, nk - 1 + nb - 2)
 
@@ -195,6 +211,13 @@
     to_mate(swap_s, swap_r, 0, swap_r)
 
     to_mate(sq_s, sq_m, 18, sq_m)
+    for k in range(nu):
+        for core in range(2):
+            peer = chips[k] * 2 + core
+            remote(send_u.at[peer], recv_u.at[k, c], 21, peer)
+            remote(sq_s, sq_u.at[k, c], 22, peer)
+    going[21] = coming[21] = recv_u
+    going[22] = coming[22] = sq_u
     to_mate(x_in, tok2.at[c], 2, x_in)
     to_mate(gain2_hbm, gain2.at[:, my_rows], 3, gain_in)
     to_mate(wo_hbm.at[other_head], wo_in.at[:, my_rows], 4, x_in)
@@ -209,14 +232,14 @@
         send_a[j] = part[c, j * seqs : (j + 1) * seqs, :].astype(BF16)
     recv_a[me] = send_a[me]
 
-    for chip in chips:
+    for chip in chips[nu:]:
         for core in range(2):
             peer = chip * 2 + core
             remote(send_a.at[peer], recv_a.at[me], 7, peer)
         remote(sq_r.at[z], sq_r.at[z], 1, chip * 2 + c)
     remote(send_a.at[mate], recv_a.at[me], 7, mate)
-    expect(nk - 1, 7, recv_a)
-    expect(nz - 1, 1, sq_r)
+    expect(nk - 1 - 2 * nu, 7, recv_a)
+    expect(nz - 1 - nu, 1, sq_r)
 
     row = lax.broadcasted_iota(jnp.int32, (seqs, size), 0)
     lane = lax.broadcasted_iota(jnp.int32, (seqs, size), 1)
@@ -230,11 +253,15 @@
     later[0].wait()
 
     arrived(1)
+    arrived(22)
     total_sq = jnp.sum(sq_r[...], axis=0)
+    for k in range(nu):
+        total_sq = total_sq + sq_u[k, 0] + sq_u[k, 1]
     row_sq = jnp.sum(jnp.where(lane == row + me * seqs, total_sq, 0.0), axis=1, keepdims=True)
     scale1 = lax.rsqrt(row_sq / d_model + EPS)
 
     arrived(7)
+    arrived(21)
     queries, keys, values, gates = [], [], [], []
 
     def turn(v):
@@ -244,6 +271,8 @@
         total = recv_a[h].astype(F32)
         for j in range(1, nz):
             total = total + recv_a[2 * j + h].astype(F32)
+        for k in range(nu):
+            total = total + recv_u[k, 0, h].astype(F32) + recv_u[k, 1, h].astype(F32)
         total = total * scale1
         queries.append(turn(total[:, :size]))
         keys.append(turn(total[:, size : 2 * size]) * size**-0.5)
@@ -464,6 +493,9 @@
             ((nz, 1, rows), F32),
             ((nk, seqs, 4 * size), BF16),
             ((nk, seqs, 4 * size), BF16),
+            ((nk, 2, seqs, 4 * size), BF16),
+            ((3, 2, 2, seqs, 4 * size), BF16),
+            ((3, 2, 1, rows), F32),
             ((2, seqs, size), BF16),
             ((nk, seqs, size), BF16),
             ((rows, size), F32),
@@ -496,8 +528,8 @@
             + [pltpu.VMEM(s, t) for s, t in scratch]
             + [
                 pltpu.SemaphoreType.DMA((14,)),
-                pltpu.SemaphoreType.DMA((20,)),
-                pltpu.SemaphoreType.DMA((20,)),
+                pltpu.SemaphoreType.DMA((23,)),
+                pltpu.SemaphoreType.DMA((23,)),
                 pltpu.SemaphoreType.DMA((nr,)),
                 pltpu.SemaphoreType.DMA((nr + 1,)),
             ],

time: 110 us -> 110 us (level)
  no operation moved by 1% of the time
where the time goes in v9:
time: 110 us
  Pallas kernels  108 us (98%)
  local copies, waits for them, and re-layouts  1.41 us (1%)
    pallas_call x1, Pallas kernels, shards(): pl.pallas_call(functools.partial(kernel, cfg), out_shape=(pltpu.VMEM((row...  108 us

profile of v9, /device:TPU:65, one launch (start us, length us, event | category | flops | bytes accessed | tf_op | source)
XLA Modules:
  0.0 110.0 jit_solution(2351172791981042591)
XLA Ops:
  0.6 108.0 %step.1 = (bf16[128,128]{1,0:T(8,128)(2,1)S(1)}, f32[4,2,128,128]{3,2,1,0:T(8,128)S(1)}) custom-call(s32[4]{0:T(128)} %pos_hbm.1, bf16[128,128]{1,0:T(8,128)(2,1)} %x_hbm.1, f32[4,2,128,128]{3,2,1,0:T(8,128)} %state_hbm.1, f32[1,128]{1,0:T(1,128)} %bitcast.2, bf16[128,256]{1,0:T(8,128)(2,1)} %wq_hbm.1, bf16[128,256]{1,0:T(8,128)(2,1)} %wk_hbm.1, ...), custom_call_target="tpu_custom_call" | custom-call | tf_op jit(solution)/shard_map/step/pallas_call | solution.py:519
  108.6 0.6 copy.17
  109.2 0.8 copy.18

commit v10 on v8

--- a/solution.py
+++ b/solution.py
@@ -129,12 +129,10 @@
 
     here = pl.ds(pl.multiple_of(c * half_ff, 128), half_ff)
     there = pl.ds(pl.multiple_of((1 - c) * half_ff, 128), half_ff)
-    mine = pl.ds(pl.multiple_of(c * size, 128), size)
-    other_head = pl.ds(pl.multiple_of((1 - c) * size, 128), size)
     my_rows = pl.ds(pl.multiple_of(c * width, 128), width)
     later = [
         load(state_hbm, state_in, 6),
-        load(wo_hbm.at[mine], wo_in.at[:, my_rows], 7),
+        load(wo_hbm, wo_in.at[:, my_rows], 7),
         load(gain2_hbm, gain2.at[:, my_rows], 8),
         load(wu_hbm.at[:, here], wu_in.at[my_rows], 9),
         load(wd_hbm.at[here], wd_in.at[:, my_rows], 10),
@@ -197,7 +195,13 @@
     to_mate(sq_s, sq_m, 18, sq_m)
     to_mate(x_in, tok2.at[c], 2, x_in)
     to_mate(gain2_hbm, gain2.at[:, my_rows], 3, gain_in)
-    to_mate(wo_hbm.at[other_head], wo_in.at[:, my_rows], 4, x_in)
+
+    @pl.when(c == 0)
+    def _():
+        remote(wo_hbm, wo_in.at[:, my_rows], 4, mate)
+
+    going[4] = (wo_in.at[:, pl.ds(0, width)], None)
+    coming[4] = (None, wo_in.at[:, pl.ds(0, width)])
     to_mate(wu_hbm.at[:, there], wu_in.at[my_rows], 5, wu_in.at[pl.ds(0, width)])
     to_mate(wd_hbm.at[there], wd_in.at[:, my_rows], 6, wd_in.at[:, pl.ds(0, width)])
 
@@ -267,12 +271,20 @@
         read = jnp.concatenate(reads, axis=0)
         read = read * lax.rsqrt(jnp.mean(read * read, axis=1, keepdims=True) + EPS)
         gate = gates[h]
-        ret_s[h] = (read * (gate / (1.0 + jnp.exp(-gate)))).astype(BF16)
-    ret_r[me] = ret_s[c]
-
-    for peer, core in kv_peers:
-        remote(ret_s.at[core], ret_r.at[me], 8, peer)
-    expect(nk - 1, 8, ret_r)
+        ret_s[:, h * size : (h + 1) * size] = (read * (gate / (1.0 + jnp.exp(-gate)))).astype(BF16)
+    for chip in chips:
+        remote(ret_s, ret_r.at[me], 8, chip * 2 + 1)
+
+    @pl.when(c == 0)
+    def _():
+        remote(ret_s, ret_r.at[me], 8, mate)
+
+    @pl.when(c == 1)
+    def _():
+        ret_r[me] = ret_s[...]
+
+    going[8] = (ret_r.at[pl.ds(0, nz)], ret_r.at[pl.ds(0, nz - 1)])
+    coming[8] = (None, ret_r.at[pl.ds(0, nk - 1)])
 
     later[1].wait()
     later[2].wait()
@@ -286,9 +298,18 @@
             ].astype(F32)
 
     arrived(8)
-    for j in range(nk):
-        ret_f[j * seqs : (j + 1) * seqs] = ret_r[j].astype(F32)
-    terms = jnp.dot(ret_f[...].astype(BF16), wo_in[...], preferred_element_type=F32)
+    @pl.when(c == 1)
+    def _():
+        for j in range(nk):
+            ret_f[j * seqs : (j + 1) * seqs] = ret_r[j].astype(F32)
+        head_terms = jnp.dot(ret_f[...].astype(BF16), wo_in[...], preferred_element_type=F32)
+        send_c[0] = head_terms.reshape(nt, group, 2 * width).astype(BF16)
+        for t in columns_x:
+            remote(send_c.at[0, t], recv_c.at[0, tp], 9, me, t)
+        recv_c[0, tp] = send_c[0, tp]
+
+    going[9] = (None, send_c.at[0, pl.ds(0, nt - 1)])
+    coming[9] = (None, recv_c.at[0, pl.ds(0, nt - 1)])
 
     def send_sums(which, phase):
         send_c[which] = terms.reshape(nt, group, 2 * width).astype(BF16)
@@ -307,14 +328,11 @@
         going[phase] = (send_c.at[which], send_c.at[which, pl.ds(0, nt - 1)])
         coming[phase] = (None, recv_c.at[which, pl.ds(0, nb - 1)])
 
-    def added(which):
-        return jnp.sum(recv_c[which].astype(F32), axis=0)
-
-    send_sums(0, 9)
     arrived(9)
     @pl.when(c == 1)
     def _():
-        mixed = (tok_rows[tp] + added(0)).astype(BF16)
+        added = jnp.sum(recv_c[0, :nt].astype(F32), axis=0)
+        mixed = (tok_rows[tp] + added).astype(BF16)
         mix_s[...] = mixed
         mix_r[tp] = mixed
         for t in columns_x:
@@ -398,7 +416,8 @@
     arrived(14)
     @pl.when(c == 1)
     def _():
-        final = (mix_s[...].astype(F32) + added(1)).astype(BF16)
+        added = jnp.sum(recv_c[1].astype(F32), axis=0)
+        final = (mix_s[...].astype(F32) + added).astype(BF16)
         for s in range(2):
             out_s[s] = final[:, s * width : (s + 1) * width]
         out_r[tp] = out_s[1]
@@ -451,7 +470,7 @@
             ((1, width), F32),
             ((4, width, heads * size), BF16),
             (state.shape, F32),
-            ((size, 2 * width), BF16),
+            ((heads * size, 2 * width), BF16),
             ((2 * width, ff // 2), BF16),
             ((ff // 2, 2 * width), BF16),
             ((2, rows, width), BF16),
@@ -464,9 +483,9 @@
             ((nz, 1, rows), F32),
             ((nk, seqs, 4 * size), BF16),
             ((nk, seqs, 4 * size), BF16),
-            ((2, seqs, size), BF16),
-            ((nk, seqs, size), BF16),
-            ((rows, size), F32),
+            ((seqs, heads * size), BF16),
+            ((nk, seqs, heads * size), BF16),
+            ((rows, heads * size), F32),
             ((2, nt, group, 2 * width), BF16),
             ((2, nb, group, 2 * width), BF16),
             ((nt, group, 2 * width), F32),

time: 110 us -> 108 us (0.982)
    pallas_call x1, Pallas kernels: 107 us -> 106 us  [shards(): pl.pallas_call(functools.partial(kernel, cfg), out_shape=(pltpu.VMEM((row...]
where the time goes in v10:
time: 108 us
  Pallas kernels  106 us (98%)
  local copies, waits for them, and re-layouts  1.41 us (1%)
    pallas_call x1, Pallas kernels, shards(): pl.pallas_call(functools.partial(kernel, cfg), out_shape=(pltpu.VMEM((row...  106 us

profile of v10, /device:TPU:65, one launch (start us, length us, event | category | flops | bytes accessed | tf_op | source)
XLA Modules:
  0.0 108.3 jit_solution(13807077890485673941)
XLA Ops:
  0.6 106.3 %step.1 = (bf16[128,128]{1,0:T(8,128)(2,1)S(1)}, f32[4,2,128,128]{3,2,1,0:T(8,128)S(1)}) custom-call(s32[4]{0:T(128)} %pos_hbm.1, bf16[128,128]{1,0:T(8,128)(2,1)} %x_hbm.1, f32[4,2,128,128]{3,2,1,0:T(8,128)} %state_hbm.1, f32[1,128]{1,0:T(1,128)} %bitcast.2, bf16[128,256]{1,0:T(8,128)(2,1)} %wq_hbm.1, bf16[128,256]{1,0:T(8,128)(2,1)} %wk_hbm.1, ...), custom_call_target="tpu_custom_call" | custom-call | tf_op jit(solution)/shard_map/step/pallas_call | solution.py:506
  106.9 0.6 copy.17
  107.5 0.8 copy.18

commit v11 on v10

--- a/solution.py
+++ b/solution.py
@@ -110,6 +110,11 @@
         copy.start()
         return copy
 
+    def greet(peers):
+        for peer, _ in peers:
+            pl.semaphore_signal(barrier, inc=1, device_id={"kv": peer}, device_id_type=MESH)
+
+    greet(kv_peers[:6])
     first = [
         load(x_hbm, x_in, 0),
         load(gain_hbm, gain_in, 1),
@@ -120,8 +125,7 @@
         load(pos_hbm, pos_ref, 12),
         load(freq_hbm, freq_ref, 13),
     ]
-    for peer, _ in kv_peers:
-        pl.semaphore_signal(barrier, inc=1, device_id={"kv": peer}, device_id_type=MESH)
+    greet(kv_peers[6:])
     for t, core in block_peers[:-1]:
         pl.semaphore_signal(
             barrier, inc=1, device_id={"kv": z * 2 + core, "tp": t}, device_id_type=MESH
@@ -142,14 +146,11 @@
         copy.wait()
     x = x_in[...].astype(F32)
     normed = (x * gain_in[...]).astype(BF16)
-    square = x * x
-    sq_s[...] = jnp.sum(jnp.transpose(square), axis=0, keepdims=True)
     for n in range(4):
         both = jnp.dot(normed, w_in[n], preferred_element_type=F32)
         part[0, :, n * size : (n + 1) * size] = both[:, :size]
         part[1, :, n * size : (n + 1) * size] = both[:, size:]
     swap_s[...] = part[1 - c].astype(BF16)
-    tok2[c] = x_in[...]
 
     pl.semaphore_wait(barrier, nk - 1 + nb - 2)
 
@@ -192,6 +193,9 @@
 
     to_mate(swap_s, swap_r, 0, swap_r)
 
+    square = x_in[...].astype(F32)
+    square = square * square
+    sq_s[...] = jnp.sum(jnp.transpose(square), axis=0, keepdims=True)
     to_mate(sq_s, sq_m, 18, sq_m)
     to_mate(x_in, tok2.at[c], 2, x_in)
     to_mate(gain2_hbm, gain2.at[:, my_rows], 3, gain_in)
@@ -289,6 +293,7 @@
     later[1].wait()
     later[2].wait()
     arrived(2)
+    tok2[c] = x_in[...]
     arrived(3)
     arrived(4)
     for m in range(nt):
@@ -346,15 +351,6 @@
     arrived(5)
     arrived(10)
     middle = mix_r[...].astype(F32).reshape(rows, 2 * width)
-    square = middle * middle
-    sq2_s[...] = jnp.sum(
-        jnp.transpose(square[:, :width] + square[:, width:]), axis=0, keepdims=True
-    )
-    sq2_r[z] = sq2_s[...]
-
-    for chip in chips:
-        remote(sq2_s, sq2_r.at[z], 11, chip * 2 + c)
-    expect(nz - 1, 11, sq2_r)
     normed2 = (middle * gain2[...]).astype(BF16)
     upward = jnp.dot(normed2, wu_in[...], preferred_element_type=F32)
     send_d[...] = upward.reshape(nz, per_chip, half_ff).astype(BF16)
@@ -376,6 +372,15 @@
         hop(send_d.at[ring(left + offset, nz)], near_d.at[k, 1], left * 2 + c, 12, near_sem.at[k])
     going[12] = send_d.at[pl.ds(0, 2 * nr)]
     hop(send_d.at[z], recv_d.at[nr], mate, 19, far_sem.at[0])
+    square = middle * middle
+    sq2_s[...] = jnp.sum(
+        jnp.transpose(square[:, :width] + square[:, width:]), axis=0, keepdims=True
+    )
+    sq2_r[z] = sq2_s[...]
+
+    for chip in chips:
+        remote(sq2_s, sq2_r.at[z], 11, chip * 2 + c)
+    expect(nz - 1, 11, sq2_r)
     for k, offset in enumerate(relayed):
         target = ring(z + offset, nz)
         pltpu.make_async_copy(near_d.at[k], near_d.at[k], near_sem.at[k]).wait()

time: 108 us -> 108 us (level)
  no operation moved by 1% of the time
where the time goes in v11:
time: 108 us; the launch traced here: 107 us
  Pallas kernels  105 us (97%)
  local copies, waits for them, and re-layouts  1.41 us (1%)
    pallas_call x1, Pallas kernels, shards(): pl.pallas_call(functools.partial(kernel, cfg), out_shape=(pltpu.VMEM((row...  105 us

profile of v11, /device:TPU:65, one launch (start us, length us, event | category | flops | bytes accessed | tf_op | source)
XLA Modules:
  0.0 107.5 jit_solution(10204150290291348264)
XLA Ops:
  0.6 105.4 %step.1 = (bf16[128,128]{1,0:T(8,128)(2,1)S(1)}, f32[4,2,128,128]{3,2,1,0:T(8,128)S(1)}) custom-call(s32[4]{0:T(128)} %pos_hbm.1, bf16[128,128]{1,0:T(8,128)(2,1)} %x_hbm.1, f32[4,2,128,128]{3,2,1,0:T(8,128)} %state_hbm.1, f32[1,128]{1,0:T(1,128)} %bitcast.2, bf16[128,256]{1,0:T(8,128)(2,1)} %wq_hbm.1, bf16[128,256]{1,0:T(8,128)(2,1)} %wk_hbm.1, ...), custom_call_target="tpu_custom_call" | custom-call | tf_op jit(solution)/shard_map/step/pallas_call | solution.py:511
  106.1 0.6 copy.17
  106.7 0.8 copy.18

commit v12 on v11

--- a/solution.py
+++ b/solution.py
@@ -438,6 +438,15 @@
     out_ref[...] = out_r[...].reshape(rows, width)
 
 
+def deliver(layer_ref, state_ref, layer_out, state_out, sem):
+    first = pltpu.make_async_copy(state_ref, state_out, sem.at[0])
+    second = pltpu.make_async_copy(layer_ref, layer_out, sem.at[1])
+    first.start()
+    second.start()
+    first.wait()
+    second.wait()
+
+
 def solution(mesh):
     nk, nt = mesh.shape["kv"], mesh.shape["tp"]
     nz = nk // 2
@@ -508,7 +517,7 @@
             ((2, group, width), BF16),
             ((nt, group, width), BF16),
         ]
-        return pl.pallas_call(
+        layer, new_state = pl.pallas_call(
             functools.partial(kernel, cfg),
             out_shape=(
                 pltpu.VMEM((rows, width), BF16),
@@ -544,6 +553,20 @@
             w_down,
             freq,
         )
+        return pl.pallas_call(
+            deliver,
+            out_shape=(
+                jax.ShapeDtypeStruct(layer.shape, BF16),
+                jax.ShapeDtypeStruct(state.shape, F32),
+            ),
+            in_specs=[vmem, vmem],
+            out_specs=(anywhere, anywhere),
+            scratch_shapes=[pltpu.SemaphoreType.DMA((2,))],
+            name="deliver",
+        )(
+            pltpu.with_memory_space_constraint(layer, pltpu.VMEM),
+            pltpu.with_memory_space_constraint(new_state, pltpu.VMEM),
+        )
 
     return jax.shard_map(
         shards,

time: 108 us -> 107 us (level)
  local copies, waits for them, and re-layouts: 1.41 us -> 0 us
    unnamed x2 -> x0, local copies, waits for them, and re-layouts: 1.41 us -> none
where the time goes in v12:
time: 107 us
  Pallas kernels  106 us (99%)
    pallas_call x1, Pallas kernels, shards(): pl.pallas_call(functools.partial(kernel, cfg), out_shape=(pltpu.VMEM((row...  106 us

profile of v12, /device:TPU:65, one launch (start us, length us, event | category | flops | bytes accessed | tf_op | source)
XLA Modules:
  0.0 107.0 jit_solution(295596546744485347)
XLA Ops:
  0.6 105.5 %step.1 = (bf16[128,128]{1,0:T(8,128)(2,1)S(1)}, f32[4,2,128,128]{3,2,1,0:T(8,128)S(1)}) custom-call(s32[4]{0:T(128)} %pos_hbm.1, bf16[128,128]{1,0:T(8,128)(2,1)} %x_hbm.1, f32[4,2,128,128]{3,2,1,0:T(8,128)} %state_hbm.1, f32[1,128]{1,0:T(1,128)} %bitcast.2, bf16[128,256]{1,0:T(8,128)(2,1)} %wq_hbm.1, bf16[128,256]{1,0:T(8,128)(2,1)} %wk_hbm.1, ...), custom_call_target="tpu_custom_call" | custom-call | tf_op jit(solution)/shard_map/step/pallas_call | solution.py:520
  106.1 0.8 deliver.1
